TPU v7x, 256 devices: a whole 4x4x8 slice. The times are simulated.
256 devices in a mesh: sp: 64 (over z, x, core), tp: 4 (over y).
Axes of the slice: x: 4, y: 4, z: 8, core: 2. Of those that a mesh axis runs over, the one named last changes fastest.
Arguments:
- conv_value: bfloat16 [32768, 1024], P('sp', 'tp'), may hold values from -6 to 6
- conv_gate: bfloat16 [32768, 1024], P('sp', 'tp'), may hold values from -9 to 9
- conv_weight: float32 [31, 1024], P(None, 'tp'), may hold values from -2.2 to 2.2
- conv_gain: float32 [1024], P('tp'), may hold values from 0.1 to 1.9
- conv_shift: float32 [1024], P('tp'), may hold values from -3 to 3
- out_weight: bfloat16 [1024, 2048], P('tp'), may hold values from -0.1875 to 0.1875
- residual: bfloat16 [32768, 2048], P('sp', 'tp'), may hold values from -10 to 10
- mix_gain: float32 [2048], P('tp'), may hold values from 0.1 to 1.9
- expert_ids: int32 [32768, 2], P('sp'), may hold values from 0 to 63, all different within a row; in each aligned block of 128 rows (0 to 127, 128 to 255, ...) at most 8 rows name the same one
- group_weight: float32 [32768], P('sp'), may hold values from 0.6 to 1
- score_gap: float32 [32768], P('sp'), may hold values from -0.8 to 0.8
- w_gate: bfloat16 [64, 2048, 1024], P('sp', None, 'tp'), may hold values from -0.125 to 0.125
- w_up: bfloat16 [64, 2048, 1024], P('sp', None, 'tp'), may hold values from -0.125 to 0.125
- w_down: bfloat16 [64, 1024, 2048], P('sp', 'tp'), may hold values from -0.1875 to 0.1875
Outputs:
- layer_out: bfloat16 [32768, 2048], P('sp', 'tp')
Inputs may be any that keep to these rules, and one draw needn't show every extreme that they name: `expert_ids`: the two experts of a position differ. In each aligned block of 512 // 4 positions no expert is named by more than 8 rows, a bound that some block reaches.
All inputs are finite; a program needn't handle non-finite values.
Results may differ from a plain program's by a relative error of at most 0.012.
Values may be sent and summed in bfloat16 or wider, within the bound.
A program may use at most 128 MiB of HBM per device.

v0:
```python
import jax
import jax.numpy as jnp
from jax import lax
from jax.sharding import PartitionSpec as P

D = 2048
CH = 1024


eps = 1e-06


def passed_along(value, axis, steps):
    count = lax.axis_size(axis)
    leading, last = (max(0, -steps), min(count, count - steps))
    return lax.ppermute(value, axis, [(source, source + steps) for source in range(leading, last)])


def from_everyone(shard, axis):
    copies = jnp.broadcast_to(shard, (lax.axis_size(axis), *shard.shape))
    return lax.all_to_all(copies, axis, split_axis=0, concat_axis=0, tiled=True)


def of_everyone(shard, axis):
    everything = from_everyone(shard, axis)
    return jnp.sum(everything, axis=0)


def together(arrays, axis):
    vector, at, outs = (jnp.concatenate([a.reshape(-1) for a in arrays]), 0, [])
    subtotal = of_everyone(vector, axis)
    for a in arrays:
        outs.append(subtotal[at : at + a.size].reshape(a.shape))
        at += a.size
    return tuple(outs)


def in_blocks(shard, dim, count):
    before, after = (shard.shape[:dim], shard.shape[dim + 1 :])
    return jnp.moveaxis(shard.reshape(*before, count, -1, *after), dim, 0)


def sum_at_owner(shard, axis, dim):
    count = lax.axis_size(axis)
    pieces = lax.all_to_all(in_blocks(shard, dim, count), axis, 0, 0, tiled=True)
    return jnp.sum(pieces.astype(jnp.float32), axis=0)


def shards(
    conv_value,
    conv_gate,
    conv_weight,
    conv_gain,
    conv_shift,
    out_weight,
    residual,
    mix_gain,
    expert_ids,
    group_weight,
    score_gap,
    w_gate,
    w_up,
    w_down,
):
    row_count = conv_value.shape[0]
    reach_rows = conv_weight.shape[0] - 1
    seq_devices = lax.axis_size("sp")
    tp_devices = lax.axis_size("tp")
    prev_value, prev_gate = passed_along(
        (conv_value[row_count - reach_rows :], conv_gate[row_count - reach_rows :]), "sp", 1
    )
    values = jnp.concatenate([prev_value, conv_value], axis=0).astype(jnp.float32)
    gate_pre = jnp.concatenate([prev_gate, conv_gate], axis=0).astype(jnp.float32)
    gated = values * jax.nn.sigmoid(gate_pre)
    convolved = jnp.zeros((row_count, conv_value.shape[1]), jnp.float32)
    for tap_index in range(reach_rows + 1):
        convolved = convolved + conv_weight[tap_index] * gated[tap_index : tap_index + row_count]
    row_sum, squares = together(
        (jnp.sum(convolved, axis=-1), jnp.sum(convolved * convolved, axis=-1)), "tp"
    )
    row_mean = (row_sum / CH)[:, None]
    row_var = (squares / CH)[:, None] - row_mean * row_mean
    normalized = (convolved - row_mean) * lax.rsqrt(row_var + eps) * conv_gain + conv_shift
    activated = jax.nn.silu(normalized).astype(jnp.bfloat16)
    partial_out = jnp.dot(activated, out_weight, preferred_element_type=jnp.float32)
    mixed = sum_at_owner(partial_out.astype(jnp.bfloat16), "tp", 1)
    middle = (residual.astype(jnp.float32) + mixed).astype(jnp.bfloat16)
    middle_wide = middle.astype(jnp.float32)
    row_sq = of_everyone(jnp.sum(middle_wide * middle_wide, axis=-1), "tp")
    normed = (middle_wide * lax.rsqrt(row_sq / D + eps)[:, None] * mix_gain).astype(jnp.bfloat16)
    quarter = row_count // tp_devices
    capacity = 4 * quarter // seq_devices
    expert_num = expert_ids.reshape(tp_devices, quarter * 2)
    onehot = (
        expert_num[:, :, None] == jnp.arange(seq_devices, dtype=jnp.int32)[None, None, :]
    ).astype(jnp.int32)
    before = jnp.cumsum(onehot, axis=1) - onehot
    ranking = jnp.sum(before * onehot, axis=-1)
    quarter_index = jnp.arange(tp_devices, dtype=jnp.int32)[:, None]
    slots = ((expert_num * tp_devices + quarter_index) * capacity + ranking).reshape(-1)
    own_rows = lax.all_to_all(normed, "tp", split_axis=0, concat_axis=1, tiled=True)
    my_index = lax.axis_index("tp")
    own_experts = lax.dynamic_slice_in_dim(expert_num, my_index, 1, 0)[0]
    own_rank = lax.dynamic_slice_in_dim(ranking, my_index, 1, 0)[0]
    own_slots = own_experts * capacity + own_rank
    token_of = jnp.arange(quarter * 2, dtype=jnp.int32) // 2
    outgoing = (
        jnp.zeros((seq_devices * capacity, D), jnp.bfloat16).at[own_slots].set(own_rows[token_of])
    )
    received = lax.all_to_all(
        outgoing.reshape(seq_devices, capacity, D), "sp", split_axis=0, concat_axis=0, tiled=True
    )
    gathered = lax.all_gather(received[:, None], "tp", axis=1, tiled=True)
    expert_in = gathered.reshape(-1, D)
    gate_part = jnp.dot(expert_in, w_gate[0], preferred_element_type=jnp.float32)
    up_part = jnp.dot(expert_in, w_up[0], preferred_element_type=jnp.float32)
    hidden = (jax.nn.silu(gate_part) * up_part).astype(jnp.bfloat16)
    partial_value = jnp.dot(hidden, w_down[0], preferred_element_type=jnp.float32)
    columns = lax.psum_scatter(
        partial_value.astype(jnp.bfloat16), "tp", scatter_dimension=1, tiled=True
    )
    col_count = columns.shape[1]
    returned = lax.all_to_all(
        columns.reshape(seq_devices, tp_devices * capacity, col_count),
        "sp",
        split_axis=0,
        concat_axis=0,
        tiled=True,
    )
    lookup = returned.reshape(-1, col_count)
    col_count = lookup.shape[1]
    picked = lookup[slots].reshape(row_count, 2, col_count).astype(jnp.float32)
    first_gate = group_weight * jax.nn.sigmoid(score_gap)
    second_gate = group_weight * jax.nn.sigmoid(-score_gap)
    result = middle_wide + first_gate[:, None] * picked[:, 0] + second_gate[:, None] * picked[:, 1]
    return result.astype(jnp.bfloat16)


def solution(mesh):
    return jax.shard_map(
        shards,
        mesh=mesh,
        in_specs=(
            P("sp", "tp"),
            P("sp", "tp"),
            P(None, "tp"),
            P("tp"),
            P("tp"),
            P("tp", None),
            P("sp", "tp"),
            P("tp"),
            P("sp", None),
            P("sp"),
            P("sp"),
            P("sp", None, "tp"),
            P("sp", None, "tp"),
            P("sp", "tp", None),
        ),
        out_specs=P("sp", "tp"),
        check_vma=False,
    )
```

profile of v0, /device:TPU:24, one launch (start us, length us, event | category | flops | bytes accessed | tf_op | source)
XLA Modules:
  0.0 414.8 jit_solution(11208760624658527416)
XLA Ops:
  7.3 1.7 collective-permute-start
  9.8 3.7 collective-permute-start.1
  15.5 1.2 divide_multiply_fusion
  16.8 2.4 fusion.60
  19.2 7.8 %all_to_all.46 = f32[4,1,1024]{2,1,0:T(1,128)S(1)} all-to-all(f32[4,1,1024]{2,1,0:T(1,128)S(1)} %broadcast_in_dim.8), channel_id=1, replica_groups=mesh['sp'=64,'tp'=4] {'tp'}, dimensions={0} | all-to-all | bytes 32768 | tf_op jit(solution)/shard_map/all_to_all | solution.py:21
  27.9 1.6 copy.82
  29.4 5.8 %all-to-all-start.1 = ((bf16[4,512,512]{2,1,0:T(8,128)(2,1)}), bf16[4,512,512]{2,1,0:T(8,128)(2,1)S(1)}, u32[]{:S(2)}, u32[]{:S(2)}) async-start(bf16[4,512,512]{2,1,0:T(8,128)(2,1)} %bitcast.108), calls=%async_computation.1 | async-start | bytes 4194304 | tf_op jit(solution)/shard_map/all_to_all | solution.py:45
  36.8 4.5 %reduce-window.6 = s32[4,64,2,128]{3,1,2,0:T(8,128)S(1)} reduce-window(s32[4,64,2,128]{3,1,2,0:T(8,128)} %fusion.55, s32[]{:T(128)} %constant.29.clone.1), window={size=1x1x1x128 pad=0_0x0_0x0_0x127_0}, to_apply=%region_4.5 | reduce-window | flops 8323072 | bytes 524292 | tf_op jit(solution)/shard_map/reduce-window
  43.2 15.3 %all-to-all-done.1 = bf16[4,512,512]{2,1,0:T(8,128)(2,1)S(1)} async-done(((bf16[4,512,512]{2,1,0:T(8,128)(2,1)}), bf16[4,512,512]{2,1,0:T(8,128)(2,1)S(1)}, u32[]{:S(2)}, u32[]{:S(2)}) %all-to-all-start.1) | async-done | bytes 2097184 | tf_op jit(solution)/shard_map/all_to_all | solution.py:45
  60.4 5.3 %all-to-all-start.2 = ((f32[4,1,512]{2,1,0:T(1,128)}), f32[4,1,512]{2,1,0:T(1,128)S(1)}, u32[]{:S(2)}, u32[]{:S(2)}) async-start(f32[4,1,512]{2,1,0:T(1,128)} %broadcast_in_dim.10), calls=%async_computation.2 | async-start | bytes 16384 | tf_op jit(solution)/shard_map/all_to_all | solution.py:21
  65.7 3.2 all-to-all-done.2
  70.0 5.5 %all-to-all-start.3 = ((bf16[4,128,512]{2,1,0:T(8,128)(2,1)}), bf16[4,128,512]{2,1,0:T(8,128)(2,1)S(1)}, u32[]{:S(2)}, u32[]{:S(2)}) async-start(bf16[4,128,512]{2,1,0:T(8,128)(2,1)} %bitcast.36), calls=%async_computation.3 | async-start | bytes 1048576 | tf_op jit(solution)/shard_map/all_to_all | solution.py:101
  75.9 5.6 %all-to-all-done.3 = bf16[4,128,512]{2,1,0:T(8,128)(2,1)S(1)} async-done(((bf16[4,128,512]{2,1,0:T(8,128)(2,1)}), bf16[4,128,512]{2,1,0:T(8,128)(2,1)S(1)}, u32[]{:S(2)}, u32[]{:S(2)}) %all-to-all-start.3) | async-done | bytes 524320 | tf_op jit(solution)/shard_map/all_to_all | solution.py:101
  82.4 6.2 %scatter_custom_fusion = bf16[512,2048]{1,0:T(8,128)(2,1)S(1)} fusion(s32[256]{0:T(256)S(1)} %bitcast.150, bf16[128,2048]{1,0:T(8,128)(2,1)} %bitcast.113, s32[1024]{0:T(1024)S(1)} %pad_clamp_fusion, bf16[]{:T(256)} %constant.25.clone.1), kind=kCustom, calls=%fused_computation.25 | custom fusion | bytes 2097664 | tf_op jit(solution)/shard_map/scatter | solution.py:108
  88.6 62.9 %all_to_all.47 = bf16[64,8,2048]{2,1,0:T(8,128)(2,1)} all-to-all(bf16[64,8,2048]{2,1,0:T(8,128)(2,1)S(1)} %bitcast.109), channel_id=1, replica_groups=mesh['sp'=64,'tp'=4] {'sp'}, dimensions={0} | all-to-all | bytes 4194304 | tf_op jit(solution)/shard_map/all_to_all | solution.py:110
  151.7 80.3 %all-gather.3.cloned.1.call-done = bf16[64,32,2048]{2,1,0:T(8,128)(2,1)} async-done(((bf16[64,8,2048]{2,1,0:T(8,128)(2,1)}), bf16[64,32,2048]{2,1,0:T(8,128)(2,1)}) %all-gather.3.cloned.1.call-update) | async-done | bytes 8388624 | tf_op jit(solution)/shard_map/all_gather | solution.py:113
  232.0 7.2 %fusion.11 = f32[2048,256]{1,0:T(8,128)} fusion(bf16[2048,2048]{1,0:T(8,128)(2,1)} %bitcast.151, bf16[1,2048,256]{2,1,0:T(8,128)(2,1)S(1)} %copy-done.11), kind=kOutput, calls=%fused_computation.23 | convolution fusion | flops 2147483648 | bytes 11534336 | tf_op jit(solution)/shard_map/dot_general | solution.py:115
  239.2 13.1 %convolution_convert_fusion = bf16[2048,2048]{1,0:T(8,128)(2,1)} fusion(bf16[2048,2048]{1,0:T(8,128)(2,1)} %bitcast.152, f32[2048,256]{1,0:T(8,128)} %fusion.11, bf16[1,256,2048]{2,1,0:T(8,128)(2,1)S(1)} %copy-done, bf16[1,2048,256]{2,1,0:T(8,128)(2,1)S(1)} %copy-done.12), kind=kOutput, calls=%fused_computation.3 | convolution fusion | flops 4302307328 | bytes 20971520 | tf_op jit(solution)/shard_map/dot_general | solution.py:118
  252.3 83.6 %reduce-scatter.2.cloned.1.call-done = bf16[2048,512]{1,0:T(8,128)(2,1)} async-done(((bf16[2048,2048]{1,0:T(8,128)(2,1)}), bf16[2048,512]{1,0:T(8,128)(2,1)}) %reduce-scatter.2.cloned.1.call-update) | async-done | bytes 2097168 | tf_op jit(solution)/shard_map/reduce_scatter | solution.py:119
  335.9 10.6 %all-to-all-start.5 = ((bf16[64,32,512]{2,1,0:T(8,128)(2,1)}), bf16[64,32,512]{2,1,0:T(8,128)(2,1)S(1)}, u32[]{:S(2)}, u32[]{:S(2)}) async-start(bf16[64,32,512]{2,1,0:T(8,128)(2,1)} %bitcast.110), calls=%async_computation.6 | async-start | bytes 4194304 | tf_op jit(solution)/shard_map/all_to_all | solution.py:123
  346.9 50.9 %all-to-all-done.5 = bf16[64,32,512]{2,1,0:T(8,128)(2,1)S(1)} async-done(((bf16[64,32,512]{2,1,0:T(8,128)(2,1)}), bf16[64,32,512]{2,1,0:T(8,128)(2,1)S(1)}, u32[]{:S(2)}, u32[]{:S(2)}) %all-to-all-start.5) | async-done | bytes 2097184 | tf_op jit(solution)/shard_map/all_to_all | solution.py:123
  397.8 5.0 %gather_fusion = bf16[1024,512]{1,0:T(8,128)(2,1)} fusion(bf16[2048,512]{1,0:T(8,128)(2,1)S(1)} %bitcast.107, s32[1024]{0:T(1024)S(1)} %broadcast_clamp_fusion), kind=kCustom, calls=%fused_computation.1 | custom fusion | bytes 2101248 | tf_op jit(solution)/shard_map/gather | solution.py:132
  402.8 2.4 reshape.190
  405.2 1.6 fusion.62
  (75 shorter events, 13.8 us)
Async XLA Ops:
  6.5 232.6 %copy-start = (bf16[1,256,2048]{2,1,0:T(8,128)(2,1)S(1)}, bf16[1,256,2048]{2,1,0:T(8,128)(2,1)}, u32[]{:S(2)}) copy-start(bf16[1,256,2048]{2,1,0:T(8,128)(2,1)} %param.27) | copy-start | bytes 3145732
  7.3 8.1 %collective-permute-start = (bf16[30,256]{1,0:T(8,128)(2,1)S(1)}, bf16[30,256]{1,0:T(8,128)(2,1)S(1)}, u32[]{:S(2)}, u32[]{:S(2)}) collective-permute-start(bf16[30,256]{1,0:T(8,128)(2,1)S(1)} %slice.211), channel_id=1, source_target_pairs={{0,4},{4,8},{8,12},{12,16},{16,20},{20,24},{24,28},{28,32},{32,36}... | collective-permute-start | bytes 46088 | tf_op jit(solution)/shard_map/ppermute | solution.py:16
  9.8 5.7 %collective-permute-start.1 = (bf16[30,256]{1,0:T(8,128)(2,1)S(1)}, bf16[30,256]{1,0:T(8,128)(2,1)S(1)}, u32[]{:S(2)}, u32[]{:S(2)}) collective-permute-start(bf16[30,256]{1,0:T(8,128)(2,1)S(1)} %slice.212), channel_id=1, source_target_pairs={{0,4},{4,8},{8,12},{12,16},{16,20},{20,24},{24,28},{28,32},{32,36}... | collective-permute-start | bytes 46088 | tf_op jit(solution)/shard_map/ppermute | solution.py:16
  16.8 10.3 %copy-start.10 = (bf16[256,2048]{1,0:T(8,128)(2,1)S(1)}, bf16[256,2048]{1,0:T(8,128)(2,1)}, u32[]{:S(2)}) copy-start(bf16[256,2048]{1,0:T(8,128)(2,1)} %param.19) | copy-start | bytes 3145732
  16.8 10.3 %copy-start.13 = (f32[256]{0:T(256)S(1)}, f32[256]{0:T(256)}, u32[]{:S(2)}) copy-start(f32[256]{0:T(256)} %param.18) | copy-start | bytes 3076
  16.8 10.3 %copy-start.14 = (f32[256]{0:T(256)S(1)}, f32[256]{0:T(256)}, u32[]{:S(2)}) copy-start(f32[256]{0:T(256)} %param.17) | copy-start | bytes 3076
  29.4 5.8 %copy-start.6 = (s32[512,2]{0,1:T(2,128)S(1)}, s32[512,2]{0,1:T(2,128)}, u32[]{:S(2)}) copy-start(s32[512,2]{0,1:T(2,128)} %param.22) | copy-start | bytes 12292
  29.4 29.1 %all-to-all-start.1 = ((bf16[4,512,512]{2,1,0:T(8,128)(2,1)}), bf16[4,512,512]{2,1,0:T(8,128)(2,1)S(1)}, u32[]{:S(2)}, u32[]{:S(2)}) async-start(bf16[4,512,512]{2,1,0:T(8,128)(2,1)} %bitcast.108), calls=%async_computation.1 | async-start | bytes 4194304 | tf_op jit(solution)/shard_map/all_to_all | solution.py:45
  35.4 0.7 copy-start.3
  43.2 25.8 %copy-start.7 = (f32[512]{0:T(512)S(1)}, f32[512]{0:T(512)}, u32[]{:S(2)}) copy-start(f32[512]{0:T(512)} %param.21) | copy-start | bytes 6148
  58.5 1.0 copy-start.5
  59.5 16.0 %copy-start.4 = (s32[512,2]{1,0:T(8,128)S(1)}, s32[512,2]{1,0:T(8,128)}, u32[]{:S(2)}) copy-start(s32[512,2]{1,0:T(8,128)} %copy-done.3) | copy-start | bytes 12292
  59.8 22.6 %copy-start.1 = (bf16[512,512]{1,0:T(8,128)(2,1)}, bf16[512,512]{1,0:T(8,128)(2,1)S(1)}, u32[]{:S(2)}) copy-start(bf16[512,512]{1,0:T(8,128)(2,1)S(1)} %get-tuple-element.8) | copy-start | bytes 1572868
  60.4 8.5 %all-to-all-start.2 = ((f32[4,1,512]{2,1,0:T(1,128)}), f32[4,1,512]{2,1,0:T(1,128)S(1)}, u32[]{:S(2)}, u32[]{:S(2)}) async-start(f32[4,1,512]{2,1,0:T(1,128)} %broadcast_in_dim.10), calls=%async_computation.2 | async-start | bytes 16384 | tf_op jit(solution)/shard_map/all_to_all | solution.py:21
  70.0 11.5 %all-to-all-start.3 = ((bf16[4,128,512]{2,1,0:T(8,128)(2,1)}), bf16[4,128,512]{2,1,0:T(8,128)(2,1)S(1)}, u32[]{:S(2)}, u32[]{:S(2)}) async-start(bf16[4,128,512]{2,1,0:T(8,128)(2,1)} %bitcast.36), calls=%async_computation.3 | async-start | bytes 1048576 | tf_op jit(solution)/shard_map/all_to_all | solution.py:101
  75.5 156.5 %all-gather.3.cloned.1.call-start = ((), (), s32[]{:S(2)}) async-start(), calls=%async_computation.8 | async-start | bytes 10485760 | tf_op jit(solution)/shard_map/all_gather | solution.py:113
  151.5 80.5 %copy-start.11 = (bf16[1,2048,256]{2,1,0:T(8,128)(2,1)S(1)}, bf16[1,2048,256]{2,1,0:T(8,128)(2,1)}, u32[]{:S(2)}) copy-start(bf16[1,2048,256]{2,1,0:T(8,128)(2,1)} %param.25) | copy-start | bytes 3145732
  151.5 184.4 %reduce-scatter.2.cloned.1.call-start = ((), (), s32[]{:S(2)}) async-start(), calls=%async_computation.7 | async-start | bytes 10485760 | tf_op jit(solution)/shard_map/reduce_scatter | solution.py:119
  232.0 7.2 %copy-start.12 = (bf16[1,2048,256]{2,1,0:T(8,128)(2,1)S(1)}, bf16[1,2048,256]{2,1,0:T(8,128)(2,1)}, u32[]{:S(2)}) copy-start(bf16[1,2048,256]{2,1,0:T(8,128)(2,1)} %param.26) | copy-start | bytes 3145732
  335.9 11.0 %copy-start.8 = (f32[512]{0:T(512)S(1)}, f32[512]{0:T(512)}, u32[]{:S(2)}) copy-start(f32[512]{0:T(512)} %param.23) | copy-start | bytes 6148
  335.9 11.0 %copy-start.9 = (f32[512]{0:T(512)S(1)}, f32[512]{0:T(512)}, u32[]{:S(2)}) copy-start(f32[512]{0:T(512)} %param.24) | copy-start | bytes 6148
  335.9 61.9 %all-to-all-start.5 = ((bf16[64,32,512]{2,1,0:T(8,128)(2,1)}), bf16[64,32,512]{2,1,0:T(8,128)(2,1)S(1)}, u32[]{:S(2)}, u32[]{:S(2)}) async-start(bf16[64,32,512]{2,1,0:T(8,128)(2,1)} %bitcast.110), calls=%async_computation.6 | async-start | bytes 4194304 | tf_op jit(solution)/shard_map/all_to_all | solution.py:123
  405.2 1.6 copy-start.2
Sparse Core Ops, SparseCore 0:
  151.6 80.3 all-gather.2
  252.4 83.3 reduce-scatter.1
where the time goes:
time: 418 us; the launch traced here: 415 us
  waiting for transfers between devices  239 us (57%)
  blocking collectives  70.7 us (17%)
  starting transfers between devices  32.8 us (8%)
  local copies, waits for them, and re-layouts  25.9 us (6%)
  matrix products  21.1 us (5%)
  between operations  13.8 us (3%)
  other arithmetic  11.7 us (3%)
    reduce_scatter x1, waiting for transfers between devices, shards(): lax.psum_scatter(partial_value.astype(jnp.bfloat16), 'tp', scatter_dimens...  83.6 us
    all_gather x1, waiting for transfers between devices, shards(): gathered = lax.all_gather(received[:, None], 'tp', axis=1, tiled=True)  80.3 us
    all_to_all x1, blocking collectives, shards(): lax.all_to_all(outgoing.reshape(seq_devices, capacity, D), 'sp', split_ax...  62.9 us
    all_to_all x1, waiting for transfers between devices, shards(): lax.all_to_all(columns.reshape(seq_devices, tp_devices * capacity, col_co...  50.9 us
    all_to_all x1, waiting for transfers between devices, sum_at_owner(): lax.all_to_all(in_blocks(shard, dim, count), axis, 0, 0, tiled=True)  15.3 us
    dot_general x1, matrix products, shards(): jnp.dot(hidden, w_down[0], preferred_element_type=jnp.float32)  13.1 us
    all_to_all x1, starting transfers between devices, shards(): lax.all_to_all(columns.reshape(seq_devices, tp_devices * capacity, col_co...  10.6 us
  transfers between devices with their start and end apart: 8, of which 6 were waited for; matrix products, arithmetic and copies ran while one was open for 3% of the time, Pallas kernels for 0%

commit v1 on v0

v1 whole, which is shorter than its diff:
```python
import jax
import jax.numpy as jnp
from jax import lax
from jax.sharding import PartitionSpec as P

D = 2048
CH = 1024


eps = 1e-06


def passed_along(value, axis, steps):
    count = lax.axis_size(axis)
    leading, last = (max(0, -steps), min(count, count - steps))
    return lax.ppermute(value, axis, [(source, source + steps) for source in range(leading, last)])


def from_everyone(shard, axis):
    copies = jnp.broadcast_to(shard, (lax.axis_size(axis), *shard.shape))
    return lax.all_to_all(copies, axis, split_axis=0, concat_axis=0, tiled=True)


def shards(
    conv_value,
    conv_gate,
    conv_weight,
    conv_gain,
    conv_shift,
    out_weight,
    residual,
    mix_gain,
    expert_ids,
    group_weight,
    score_gap,
    w_gate,
    w_up,
    w_down,
):
    row_count = conv_value.shape[0]
    reach_rows = conv_weight.shape[0] - 1
    sp = lax.axis_size("sp")
    tp = lax.axis_size("tp")
    quarter = row_count // tp
    capacity = 4 * quarter // sp
    me = lax.axis_index("tp")
    out_full = lax.all_gather(out_weight, "tp", axis=0, tiled=False)
    gate_full = lax.all_gather(w_gate[0], "tp", axis=0, tiled=False)
    up_full = lax.all_gather(w_up[0], "tp", axis=0, tiled=False)
    down_full = lax.all_gather(w_down[0], "tp", axis=0, tiled=False)
    gain_full = from_everyone(mix_gain[None], "tp").reshape(-1)
    residual_q = lax.all_to_all(residual, "tp", split_axis=0, concat_axis=1, tiled=True)

    prev_value, prev_gate = passed_along(
        (conv_value[row_count - reach_rows :], conv_gate[row_count - reach_rows :]), "sp", 1
    )
    values = jnp.concatenate([prev_value, conv_value], axis=0).astype(jnp.float32)
    gate_pre = jnp.concatenate([prev_gate, conv_gate], axis=0).astype(jnp.float32)
    gated = values * jax.nn.sigmoid(gate_pre)
    convolved = jnp.zeros((row_count, conv_value.shape[1]), jnp.float32)
    for tap_index in range(reach_rows + 1):
        convolved = convolved + conv_weight[tap_index] * gated[tap_index : tap_index + row_count]
    stats = jnp.stack([jnp.sum(convolved, axis=-1), jnp.sum(convolved * convolved, axis=-1)])
    stats = jnp.sum(from_everyone(stats.reshape(1, -1), "tp"), axis=0).reshape(2, -1)
    row_mean = (stats[0] / CH)[:, None]
    row_var = (stats[1] / CH)[:, None] - row_mean * row_mean
    normalized = (convolved - row_mean) * lax.rsqrt(row_var + eps) * conv_gain + conv_shift
    activated = jax.nn.silu(normalized).astype(jnp.bfloat16)
    act_q = lax.all_to_all(activated.reshape(tp, quarter, -1), "tp", 0, 0, tiled=True)
    middle_wide = residual_q.astype(jnp.float32)
    mixed = jnp.zeros((quarter, D), jnp.float32)
    for b in range(tp):
        term = jnp.dot(act_q[b], out_full[b], preferred_element_type=jnp.float32)
        mixed = mixed + term.astype(jnp.bfloat16).astype(jnp.float32)
    middle = (middle_wide + mixed).astype(jnp.bfloat16)
    middle_wide = middle.astype(jnp.float32)
    row_sq = jnp.mean(middle_wide * middle_wide, axis=-1, keepdims=True)
    normed = (middle_wide * lax.rsqrt(row_sq + eps) * gain_full).astype(jnp.bfloat16)
    ids = lax.dynamic_slice_in_dim(expert_ids, me * quarter, quarter, 0)
    gw = lax.dynamic_slice_in_dim(group_weight, me * quarter, quarter, 0)
    gap = lax.dynamic_slice_in_dim(score_gap, me * quarter, quarter, 0)
    experts = jnp.arange(sp, dtype=jnp.int32)
    hit = [(ids[:, k : k + 1] == experts[None]).astype(jnp.bfloat16) for k in range(2)]
    both = hit[0] + hit[1]
    rows = jnp.arange(quarter)
    lower = (rows[None, :] < rows[:, None]).astype(jnp.bfloat16)
    before = jnp.dot(lower, both, preferred_element_type=jnp.float32)
    slots = jnp.arange(sp * capacity, dtype=jnp.int32)
    places = []
    for k in range(2):
        rank = jnp.sum(before * hit[k].astype(jnp.float32), axis=1).astype(jnp.int32)
        slot = ids[:, k] * capacity + rank
        places.append((slot[:, None] == slots[None, :]).astype(jnp.bfloat16))
    send = (places[0] + places[1]).T
    outgoing = jnp.dot(send, normed, preferred_element_type=jnp.float32).astype(jnp.bfloat16)
    received = lax.all_to_all(
        outgoing.reshape(sp, capacity, D), "sp", split_axis=0, concat_axis=0, tiled=True
    ).reshape(-1, D)
    total = jnp.zeros((sp * capacity, D), jnp.float32)
    for b in range(tp):
        g = jnp.dot(received, gate_full[b], preferred_element_type=jnp.float32)
        u = jnp.dot(received, up_full[b], preferred_element_type=jnp.float32)
        hidden = (jax.nn.silu(g) * u).astype(jnp.bfloat16)
        term = jnp.dot(hidden, down_full[b], preferred_element_type=jnp.float32)
        total = total + term.astype(jnp.bfloat16).astype(jnp.float32)
    returned = lax.all_to_all(
        total.astype(jnp.bfloat16).reshape(sp, capacity, D), "sp", 0, 0, tiled=True
    ).reshape(-1, D)
    picked = [jnp.dot(p, returned, preferred_element_type=jnp.float32) for p in places]
    first_gate = (gw * jax.nn.sigmoid(gap))[:, None]
    second_gate = (gw * jax.nn.sigmoid(-gap))[:, None]
    result = (middle_wide + first_gate * picked[0] + second_gate * picked[1]).astype(jnp.bfloat16)
    return lax.all_to_all(result, "tp", split_axis=1, concat_axis=0, tiled=True)


def solution(mesh):
    return jax.shard_map(
        shards,
        mesh=mesh,
        in_specs=(
            P("sp", "tp"),
            P("sp", "tp"),
            P(None, "tp"),
            P("tp"),
            P("tp"),
            P("tp", None),
            P("sp", "tp"),
            P("tp"),
            P("sp", None),
            P("sp"),
            P("sp"),
            P("sp", None, "tp"),
            P("sp", None, "tp"),
            P("sp", "tp", None),
        ),
        out_specs=P("sp", "tp"),
        check_vma=False,
    )
```

time: 418 us -> 336 us (0.80)
  blocking collectives: 70.7 us -> 11.3 us
  waiting for transfers between devices: 239 us -> 214 us
  local copies, waits for them, and re-layouts: 25.9 us -> 3.69 us
  matrix products: 21.1 us -> 38.2 us
  starting transfers between devices: 32.8 us -> 48.1 us
  other arithmetic: 11.7 us -> 4.51 us
    reduce_scatter x1 -> x0, waiting for transfers between devices: 83.6 us -> none  [shards(): lax.psum_scatter(partial_value.astype(jnp.bfloat16), 'tp', scatter_dimens...]
    all_to_all x2 -> x1, blocking collectives: 70.7 us -> 11.3 us  [shards(): return lax.all_to_all(result, 'tp', split_axis=1, concat_axis=0, tiled=True)]
    all_gather x1 -> x4, waiting for transfers between devices: 80.3 us -> 122 us  [the longest x1 52.8 us: shards(): down_full = lax.all_gather(w_down[0], 'tp', axis=0, tiled=False)]
    dot_general x3 -> x16, matrix products: 21.1 us -> 38.2 us  [the longest x4 23.4 us: shards(): term = jnp.dot(hidden, down_full[b], preferred_element_type=jnp.float32)]
    all_to_all x3 -> x4, waiting for transfers between devices: 71.8 us -> 86.1 us  [the longest x1 50.5 us: shards(): lax.all_to_all(total.astype(jnp.bfloat16).reshape(sp, capacity, D), 'sp',...]
    all_to_all x3 -> x4, starting transfers between devices: 21.8 us -> 32.6 us  [the longest x1 10.9 us: shards(): lax.all_to_all(outgoing.reshape(sp, capacity, D), 'sp', split_axis=0, con...]
    scatter x1 -> x0, local copies, waits for them, and re-layouts: 6.21 us -> none  [shards(): jnp.zeros((seq_devices * capacity, D), jnp.bfloat16).at[own_slots]]
    gather x1 -> x0, local copies, waits for them, and re-layouts: 5.05 us -> none  [shards(): picked = lookup[slots].reshape(row_count, 2, col_count).astype(jnp.float32)]
  transfers between devices with their start and end apart: 8 -> 12, of which waited for: 6 -> 10; matrix products, arithmetic and copies ran while one was open for 3% -> 6% of each run, Pallas kernels for 0% -> 0%
where the time goes in v1:
time: 336 us; the launch traced here: 333 us
  waiting for transfers between devices  214 us (64%)
  starting transfers between devices  48.1 us (14%)
  matrix products  38.2 us (11%)
  between operations  13.4 us (4%)
  blocking collectives  11.3 us (3%)
  other arithmetic  4.51 us (1%)
  local copies, waits for them, and re-layouts  3.69 us (1%)
    all_gather x1, waiting for transfers between devices, shards(): down_full = lax.all_gather(w_down[0], 'tp', axis=0, tiled=False)  52.8 us
    all_to_all x1, waiting for transfers between devices, shards(): lax.all_to_all(total.astype(jnp.bfloat16).reshape(sp, capacity, D), 'sp',...  50.5 us
    all_gather x1, waiting for transfers between devices, shards(): gate_full = lax.all_gather(w_gate[0], 'tp', axis=0, tiled=False)  36 us
    all_gather x1, waiting for transfers between devices, shards(): up_full = lax.all_gather(w_up[0], 'tp', axis=0, tiled=False)  30.3 us
    dot_general x4, matrix products, shards(): term = jnp.dot(hidden, down_full[b], preferred_element_type=jnp.float32)  23.4 us
    all_to_all x1, waiting for transfers between devices, shards(): lax.all_to_all(outgoing.reshape(sp, capacity, D), 'sp', split_axis=0, con...  15.1 us
    all_to_all x1, waiting for transfers between devices, shards(): lax.all_to_all(residual, 'tp', split_axis=0, concat_axis=1, tiled=True)  12.7 us
    all_to_all x1, blocking collectives, shards(): return lax.all_to_all(result, 'tp', split_axis=1, concat_axis=0, tiled=True)  11.3 us
  transfers between devices with their start and end apart: 12, of which 10 were waited for; matrix products, arithmetic and copies ran while one was open for 6% of the time, Pallas kernels for 0%

profile of v1, /device:TPU:24, one launch (start us, length us, event | category | flops | bytes accessed | tf_op | source)
XLA Modules:
  0.0 333.3 jit_solution(3213288565345061540)
XLA Ops:
  12.0 3.7 %collective-permute-start = (bf16[30,256]{1,0:T(8,128)(2,1)S(1)}, bf16[30,256]{1,0:T(8,128)(2,1)S(1)}, u32[]{:S(2)}, u32[]{:S(2)}) collective-permute-start(bf16[30,256]{1,0:T(8,128)(2,1)S(1)} %slice.269), channel_id=1, source_target_pairs={{0,4},{4,8},{8,12},{12,16},{16,20},{20,24},{24,28},{28,32},{32,36}... | collective-permute-start | bytes 46088 | tf_op jit(solution)/shard_map/ppermute | solution.py:16
  16.7 2.4 fusion.147
  19.8 4.7 %all-to-all-start.1 = ((f32[4,1,1024]{2,1,0:T(1,128)}), f32[4,1,1024]{2,1,0:T(1,128)S(1)}, u32[]{:S(2)}, u32[]{:S(2)}) async-start(f32[4,1,1024]{2,1,0:T(1,128)} %broadcast_in_dim.4), calls=%async_computation.1 | async-start | bytes 32768 | tf_op jit(solution)/shard_map/all_to_all | solution.py:21
  24.5 3.3 all-to-all-done.1
  27.7 5.6 %all-to-all-start = ((bf16[4,128,512]{2,1,0:T(8,128)(2,1)}), bf16[4,128,512]{2,1,0:T(8,128)(2,1)S(1)}, u32[]{:S(2)}, u32[]{:S(2)}) async-start(bf16[4,128,512]{2,1,0:T(8,128)(2,1)} %bitcast), calls=%async_computation | async-start | bytes 1048576 | tf_op jit(solution)/shard_map/all_to_all | solution.py:52
  34.4 12.7 %all-to-all-done = bf16[4,128,512]{2,1,0:T(8,128)(2,1)S(1)} async-done(((bf16[4,128,512]{2,1,0:T(8,128)(2,1)}), bf16[4,128,512]{2,1,0:T(8,128)(2,1)S(1)}, u32[]{:S(2)}, u32[]{:S(2)}) %all-to-all-start) | async-done | bytes 524320 | tf_op jit(solution)/shard_map/all_to_all | solution.py:52
  47.1 5.5 %all-to-all-start.2 = ((bf16[4,128,256]{2,1,0:T(8,128)(2,1)}), bf16[4,128,256]{2,1,0:T(8,128)(2,1)S(1)}, u32[]{:S(2)}, u32[]{:S(2)}) async-start(bf16[4,128,256]{2,1,0:T(8,128)(2,1)} %bitcast.38), calls=%async_computation.2 | async-start | bytes 524288 | tf_op jit(solution)/shard_map/all_to_all | solution.py:69
  52.8 7.7 %all-to-all-done.2 = bf16[4,128,256]{2,1,0:T(8,128)(2,1)S(1)} async-done(((bf16[4,128,256]{2,1,0:T(8,128)(2,1)}), bf16[4,128,256]{2,1,0:T(8,128)(2,1)S(1)}, u32[]{:S(2)}, u32[]{:S(2)}) %all-to-all-start.2) | async-done | bytes 262176 | tf_op jit(solution)/shard_map/all_to_all | solution.py:69
  61.1 5.3 %all-to-all-start.3 = ((f32[4,1,512]{2,1,0:T(1,128)}), f32[4,1,512]{2,1,0:T(1,128)S(1)}, u32[]{:S(2)}, u32[]{:S(2)}) async-start(f32[4,1,512]{2,1,0:T(1,128)} %broadcast_in_dim.5), calls=%async_computation.3 | async-start | bytes 16384 | tf_op jit(solution)/shard_map/all_to_all | solution.py:21
  66.4 3.0 all-gather.12.cloned.1.call-done
  73.4 2.2 fusion
  75.5 10.9 %all-to-all-start.4 = ((bf16[64,8,2048]{2,1,0:T(8,128)(2,1)}), bf16[64,8,2048]{2,1,0:T(8,128)(2,1)S(1)}, u32[]{:S(2)}, u32[]{:S(2)}) async-start(bf16[64,8,2048]{2,1,0:T(8,128)(2,1)} %fusion), calls=%async_computation.4 | async-start | bytes 4194304 | tf_op jit(solution)/shard_map/all_to_all | solution.py:96
  86.4 36.0 %all-gather.6.cloned.1.call-done = bf16[4,2048,256]{2,1,0:T(8,128)(2,1)} async-done(((bf16[1,2048,256]{2,1,0:T(8,128)(2,1)}), bf16[4,2048,256]{2,1,0:T(8,128)(2,1)}) %all-gather.6.cloned.1.call-update) | async-done | bytes 4194320 | tf_op jit(solution)/shard_map/all_gather | solution.py:48
  122.4 15.1 %all-to-all-done.4 = bf16[64,8,2048]{2,1,0:T(8,128)(2,1)S(1)} async-done(((bf16[64,8,2048]{2,1,0:T(8,128)(2,1)}), bf16[64,8,2048]{2,1,0:T(8,128)(2,1)S(1)}, u32[]{:S(2)}, u32[]{:S(2)}) %all-to-all-start.4) | async-done | bytes 2097184 | tf_op jit(solution)/shard_map/all_to_all | solution.py:96
  137.6 3.0 fusion.27
  145.1 30.3 %all-gather.8.cloned.1.call-done = bf16[4,2048,256]{2,1,0:T(8,128)(2,1)} async-done(((bf16[1,2048,256]{2,1,0:T(8,128)(2,1)}), bf16[4,2048,256]{2,1,0:T(8,128)(2,1)}) %all-gather.8.cloned.1.call-update) | async-done | bytes 4194320 | tf_op jit(solution)/shard_map/all_gather | solution.py:49
  175.4 52.8 %all-gather.10.cloned.1.call-done = bf16[4,256,2048]{2,1,0:T(8,128)(2,1)} async-done(((bf16[1,256,2048]{2,1,0:T(8,128)(2,1)}), bf16[4,256,2048]{2,1,0:T(8,128)(2,1)}) %all-gather.10.cloned.1.call-update) | async-done | bytes 4194320 | tf_op jit(solution)/shard_map/all_gather | solution.py:50
  228.2 5.4 %convolution_convert_fusion = bf16[512,2048]{1,0:T(8,128)(2,1)} fusion(bf16[64,8,2048]{2,1,0:T(8,128)(2,1)S(1)} %all-to-all-done.4, bf16[4,256,2048]{2,1,0:T(8,128)(2,1)} %all-gather.10.cloned.1.call-done, bf16[4,2048,256]{2,1,0:T(8,128)(2,1)} %all-gather.8.cloned.1.call-done, f32[512,256]{1,0:T(8,128)} %fusion.19), kind=kOutput, calls=%fused_computation.1 | convolution fusion | flops 1075576832 | bytes 6815744 | tf_op jit(solution)/shard_map/dot_general | solution.py:104
  233.6 5.4 %convolution_convert_fusion.1 = bf16[512,2048]{1,0:T(8,128)(2,1)} fusion(bf16[64,8,2048]{2,1,0:T(8,128)(2,1)S(1)} %all-to-all-done.4, bf16[4,256,2048]{2,1,0:T(8,128)(2,1)} %all-gather.10.cloned.1.call-done, bf16[4,2048,256]{2,1,0:T(8,128)(2,1)} %all-gather.8.cloned.1.call-done, f32[512,256]{1,0:T(8,128)} %fusion.23), kind=kOutput, calls=%fused_computation.2 | convolution fusion | flops 1075576832 | bytes 6815744 | tf_op jit(solution)/shard_map/dot_general | solution.py:104
  239.0 5.3 %convolution_convert_fusion.2 = bf16[512,2048]{1,0:T(8,128)(2,1)} fusion(bf16[64,8,2048]{2,1,0:T(8,128)(2,1)S(1)} %all-to-all-done.4, bf16[4,256,2048]{2,1,0:T(8,128)(2,1)} %all-gather.10.cloned.1.call-done, bf16[4,2048,256]{2,1,0:T(8,128)(2,1)} %all-gather.8.cloned.1.call-done, f32[512,256]{1,0:T(8,128)} %fusion.27), kind=kOutput, calls=%fused_computation.3 | convolution fusion | flops 1075576832 | bytes 6815744 | tf_op jit(solution)/shard_map/dot_general | solution.py:104
  244.3 7.3 %fusion.1 = bf16[64,8,2048]{2,1,0:T(8,128)(2,1)} fusion(bf16[512,2048]{1,0:T(8,128)(2,1)} %convolution_convert_fusion, bf16[512,2048]{1,0:T(8,128)(2,1)} %convolution_convert_fusion.1, bf16[512,2048]{1,0:T(8,128)(2,1)} %convolution_convert_fusion.2, bf16[4,256,2048]{2,1,0:T(8,128)(2,1)} %all-gather.10.cloned.1.call-done, ...), kind=kOutput, calls=%fused_computation.7 | convolution fusion | flops 1083965440 | bytes 13107200 | tf_op jit(solution)/shard_map/dot_general | solution.py:104
  251.6 10.6 %all-to-all-start.5 = ((bf16[64,8,2048]{2,1,0:T(8,128)(2,1)}), bf16[64,8,2048]{2,1,0:T(8,128)(2,1)S(1)}, u32[]{:S(2)}, u32[]{:S(2)}) async-start(bf16[64,8,2048]{2,1,0:T(8,128)(2,1)} %fusion.1), calls=%async_computation.5 | async-start | bytes 4194304 | tf_op jit(solution)/shard_map/all_to_all | solution.py:106
  263.0 50.5 %all-to-all-done.5 = bf16[64,8,2048]{2,1,0:T(8,128)(2,1)S(1)} async-done(((bf16[64,8,2048]{2,1,0:T(8,128)(2,1)}), bf16[64,8,2048]{2,1,0:T(8,128)(2,1)S(1)}, u32[]{:S(2)}, u32[]{:S(2)}) %all-to-all-start.5) | async-done | bytes 2097184 | tf_op jit(solution)/shard_map/all_to_all | solution.py:106
  314.7 11.3 %all_to_all.57 = bf16[128,4,512]{2,0,1:T(8,128)(2,1)S(1)} all-to-all(bf16[128,4,512]{2,0,1:T(8,128)(2,1)S(1)} %bitcast.175), channel_id=1, replica_groups=mesh['sp'=64,'tp'=4] {'tp'}, dimensions={1} | all-to-all | bytes 1048576 | tf_op jit(solution)/shard_map/all_to_all | solution.py:113
  (62 shorter events, 20.0 us)
Async XLA Ops:
  6.5 9.2 %copy-start = (s32[512,2]{0,1:T(2,128)S(1)}, s32[512,2]{0,1:T(2,128)}, u32[]{:S(2)}) copy-start(s32[512,2]{0,1:T(2,128)} %param.22) | copy-start | bytes 12292
  6.5 10.0 %copy-start.3 = (bf16[512,256]{1,0:T(8,128)(2,1)S(1)}, bf16[512,256]{1,0:T(8,128)(2,1)}, u32[]{:S(2)}) copy-start(bf16[512,256]{1,0:T(8,128)(2,1)} %param.15) | copy-start | bytes 786436
  6.5 10.0 %copy-start.2 = (bf16[512,256]{1,0:T(8,128)(2,1)S(1)}, bf16[512,256]{1,0:T(8,128)(2,1)}, u32[]{:S(2)}) copy-start(bf16[512,256]{1,0:T(8,128)(2,1)} %param.14) | copy-start | bytes 786436
  6.5 9.2 %copy-start.4 = (f32[31,256]{1,0:T(8,128)S(1)}, f32[31,256]{1,0:T(8,128)}, u32[]{:S(2)}) copy-start(f32[31,256]{1,0:T(8,128)} %param.16) | copy-start | bytes 95236
  6.5 62.8 %all-gather.12.cloned.1.call-start = ((), (), s32[]{:S(2)}) async-start(), calls=%async_computation.10 | async-start | bytes 5242880 | tf_op jit(solution)/shard_map/all_gather | solution.py:47
  7.3 115.1 %all-gather.6.cloned.1.call-start = ((), (), s32[]{:S(2)}) async-start(), calls=%async_computation.7 | async-start | bytes 5242880 | tf_op jit(solution)/shard_map/all_gather | solution.py:48
  8.0 167.4 %all-gather.8.cloned.1.call-start = ((), (), s32[]{:S(2)}) async-start(), calls=%async_computation.8 | async-start | bytes 5242880 | tf_op jit(solution)/shard_map/all_gather | solution.py:49
  8.8 219.5 %all-gather.10.cloned.1.call-start = ((), (), s32[]{:S(2)}) async-start(), calls=%async_computation.9 | async-start | bytes 5242880 | tf_op jit(solution)/shard_map/all_gather | solution.py:50
  9.5 6.4 %collective-permute-start.1 = (bf16[30,256]{1,0:T(8,128)(2,1)S(1)}, bf16[30,256]{1,0:T(8,128)(2,1)S(1)}, u32[]{:S(2)}, u32[]{:S(2)}) collective-permute-start(bf16[30,256]{1,0:T(8,128)(2,1)S(1)} %slice.270), channel_id=1, source_target_pairs={{0,4},{4,8},{8,12},{12,16},{16,20},{20,24},{24,28},{28,32},{32,36}... | collective-permute-start | bytes 46088 | tf_op jit(solution)/shard_map/ppermute | solution.py:16
  12.0 4.5 %collective-permute-start = (bf16[30,256]{1,0:T(8,128)(2,1)S(1)}, bf16[30,256]{1,0:T(8,128)(2,1)S(1)}, u32[]{:S(2)}, u32[]{:S(2)}) collective-permute-start(bf16[30,256]{1,0:T(8,128)(2,1)S(1)} %slice.269), channel_id=1, source_target_pairs={{0,4},{4,8},{8,12},{12,16},{16,20},{20,24},{24,28},{28,32},{32,36}... | collective-permute-start | bytes 46088 | tf_op jit(solution)/shard_map/ppermute | solution.py:16
  16.7 16.7 %copy-start.6 = (f32[256]{0:T(256)S(1)}, f32[256]{0:T(256)}, u32[]{:S(2)}) copy-start(f32[256]{0:T(256)} %param.18) | copy-start | bytes 3076
  16.7 16.7 %copy-start.7 = (f32[256]{0:T(256)S(1)}, f32[256]{0:T(256)}, u32[]{:S(2)}) copy-start(f32[256]{0:T(256)} %param.17) | copy-start | bytes 3076
  19.1 41.4 %copy-start.5 = (f32[512]{0:T(512)S(1)}, f32[512]{0:T(512)}, u32[]{:S(2)}) copy-start(f32[512]{0:T(512)} %param.21) | copy-start | bytes 6148
  19.8 8.0 %all-to-all-start.1 = ((f32[4,1,1024]{2,1,0:T(1,128)}), f32[4,1,1024]{2,1,0:T(1,128)S(1)}, u32[]{:S(2)}, u32[]{:S(2)}) async-start(f32[4,1,1024]{2,1,0:T(1,128)} %broadcast_in_dim.4), calls=%async_computation.1 | async-start | bytes 32768 | tf_op jit(solution)/shard_map/all_to_all | solution.py:21
  27.7 19.4 %all-to-all-start = ((bf16[4,128,512]{2,1,0:T(8,128)(2,1)}), bf16[4,128,512]{2,1,0:T(8,128)(2,1)S(1)}, u32[]{:S(2)}, u32[]{:S(2)}) async-start(bf16[4,128,512]{2,1,0:T(8,128)(2,1)} %bitcast), calls=%async_computation | async-start | bytes 1048576 | tf_op jit(solution)/shard_map/all_to_all | solution.py:52
  47.1 13.3 %all-to-all-start.2 = ((bf16[4,128,256]{2,1,0:T(8,128)(2,1)}), bf16[4,128,256]{2,1,0:T(8,128)(2,1)S(1)}, u32[]{:S(2)}, u32[]{:S(2)}) async-start(bf16[4,128,256]{2,1,0:T(8,128)(2,1)} %bitcast.38), calls=%async_computation.2 | async-start | bytes 524288 | tf_op jit(solution)/shard_map/all_to_all | solution.py:69
  61.1 12.3 %all-to-all-start.3 = ((f32[4,1,512]{2,1,0:T(1,128)}), f32[4,1,512]{2,1,0:T(1,128)S(1)}, u32[]{:S(2)}, u32[]{:S(2)}) async-start(f32[4,1,512]{2,1,0:T(1,128)} %broadcast_in_dim.5), calls=%async_computation.3 | async-start | bytes 16384 | tf_op jit(solution)/shard_map/all_to_all | solution.py:21
  69.4 3.2 copy-start.1
  75.5 62.0 %all-to-all-start.4 = ((bf16[64,8,2048]{2,1,0:T(8,128)(2,1)}), bf16[64,8,2048]{2,1,0:T(8,128)(2,1)S(1)}, u32[]{:S(2)}, u32[]{:S(2)}) async-start(bf16[64,8,2048]{2,1,0:T(8,128)(2,1)} %fusion), calls=%async_computation.4 | async-start | bytes 4194304 | tf_op jit(solution)/shard_map/all_to_all | solution.py:96
  137.6 3.0 copy-start.8
  251.6 62.0 %all-to-all-start.5 = ((bf16[64,8,2048]{2,1,0:T(8,128)(2,1)}), bf16[64,8,2048]{2,1,0:T(8,128)(2,1)S(1)}, u32[]{:S(2)}, u32[]{:S(2)}) async-start(bf16[64,8,2048]{2,1,0:T(8,128)(2,1)} %fusion.1), calls=%async_computation.5 | async-start | bytes 4194304 | tf_op jit(solution)/shard_map/all_to_all | solution.py:106
Sparse Core Ops, SparseCore 0:
  9.2 60.1 all-gather.11
  71.2 51.1 all-gather.5
  124.2 51.1 all-gather.7
  177.1 51.1 all-gather.9

commit v2 on v1

v2 whole, which is shorter than its diff:
```python
import functools

import jax
import jax.numpy as jnp
from jax import lax
from jax.experimental import pallas as pl
from jax.experimental.pallas import tpu as pltpu
from jax.sharding import PartitionSpec as P

MESH = pl.DeviceIdType.MESH
BF = jnp.bfloat16
F32 = jnp.float32
EPS = 1e-06
TAPS_PAD = 32
CHUNK = 64


def sigmoid(v):
    return jax.nn.sigmoid(v)


def kernel(
    S,
    T,
    cv,
    cg,
    cw,
    gain,
    shift,
    ow_hbm,
    res,
    mg,
    ids,
    gw,
    gap,
    wg_hbm,
    wu_hbm,
    wd_hbm,
    out,
    ow,
    wg,
    wu,
    wd,
    halo,
    gated,
    conv,
    st,
    stats,
    mv,
    part_s,
    part_r,
    res_r,
    mg_r,
    mid,
    place,
    og,
    rc,
    xb,
    hid,
    ys,
    yr,
    fin,
    loc,
    hsend,
    hrecv,
    tsend,
    trecv,
    wsend,
    wrecv,
    ssend,
    srecv,
    fsend,
    frecv,
):
    t = lax.axis_index("tp")
    s = lax.axis_index("sp")
    rows, chans = cv.shape
    taps = cw.shape[0]
    Q = rows // T
    feats = res.shape[1]
    D = feats * T
    cap = og.shape[1]
    hidden = wg.shape[2]
    slots = S * cap

    loads = [
        pltpu.make_async_copy(wg_hbm.at[0], wg.at[t], loc.at[0]),
        pltpu.make_async_copy(wu_hbm.at[0], wu.at[t], loc.at[1]),
        pltpu.make_async_copy(ow_hbm, ow, loc.at[2]),
    ]
    for c in range(T):
        loads.append(
            pltpu.make_async_copy(
                wd_hbm.at[0, :, pl.ds(c * feats, feats)], wd.at[c, t], loc.at[3 + c]
            )
        )
    for load in loads:
        load.start()

    barrier = pltpu.get_barrier_semaphore()

    @pl.loop(1, S)
    def _(k):
        pl.semaphore_signal(
            barrier, inc=1, device_id={"sp": lax.rem(s + k, S)}, device_id_type=MESH
        )

    for d in range(1, T):
        pl.semaphore_signal(
            barrier, inc=1, device_id={"tp": lax.rem(t + d, T)}, device_id_type=MESH
        )
    gated[TAPS_PAD:, :] = cv[...].astype(F32) * sigmoid(cg[...].astype(F32))
    pl.semaphore_wait(barrier, S - 1 + T - 1)

    def remote(src, dst, send, recv, axis, who):
        return pltpu.make_async_remote_copy(
            src_ref=src,
            dst_ref=dst,
            send_sem=send,
            recv_sem=recv,
            device_id={axis: who},
            device_id_type=MESH,
        )

    def tp_copy(kind, src, dst, d):
        return remote(src, dst, tsend.at[kind, d], trecv.at[kind, d], "tp", lax.rem(t + d, T))

    def half(unit, block, h):
        if unit == 0:
            n = wg.shape[1] // 2
            return wg.at[block, pl.ds(h * n, n), :]
        if unit == 1:
            n = wu.shape[1] // 2
            return wu.at[block, pl.ds(h * n, n), :]
        n = hidden // 2
        return wd.at[unit - 2, block, pl.ds(h * n, n), :]

    right, left = lax.rem(t + 1, T), lax.rem(t + T - 1, T)
    far = lax.rem(t + 2, T)

    def ring(unit, block, h, to_right, idx):
        ref = half(unit, block, h)
        return remote(
            ref, ref, wsend.at[unit, idx], wrecv.at[unit, idx], "tp", right if to_right else left
        )

    def direct(unit, h):
        for to_right in (True, False):
            ring(unit, t, h, to_right, 2 * h + (0 if to_right else 1)).start()

    def direct_wait(unit, h, from_left):
        ring(unit, left if from_left else right, h, True, 2 * h + (0 if from_left else 1)).wait_recv()

    def relay(unit):
        direct_wait(unit, 0, True)
        ring(unit, left, 0, True, 4).start()
        direct_wait(unit, 1, False)
        ring(unit, right, 1, False, 5).start()

    def near_wait(unit):
        direct_wait(unit, 1, True)
        direct_wait(unit, 0, False)

    def far_wait(unit):
        ring(unit, far, 0, True, 4).wait_recv()
        ring(unit, far, 1, True, 5).wait_recv()

    halo_copies = [
        remote(
            src.at[pl.ds(rows - TAPS_PAD, TAPS_PAD), :],
            halo.at[i],
            hsend.at[i],
            hrecv.at[i],
            "sp",
            lax.rem(s + 1, S),
        )
        for i, src in enumerate((cv, cg))
    ]
    for copy in halo_copies:
        copy.start()
    res_copies, gain_copies = [], []
    for d in range(1, T):
        peer = lax.rem(t + d, T)
        res_copies.append(tp_copy(0, res.at[pl.ds(peer * Q, Q), :], res_r.at[t], d))
        gain_copies.append(tp_copy(1, mg, mg_r.at[t], d))
    for copy in res_copies + gain_copies:
        copy.start()
    loads[0].wait()
    direct(0, 0)
    res_r[t] = res[pl.ds(t * Q, Q), :]
    mg_r[t] = mg[...]

    for copy in halo_copies:
        copy.wait_recv()
    first = jnp.where(s == 0, 0.0, 1.0).astype(F32)
    gated[:TAPS_PAD, :] = halo[0].astype(F32) * sigmoid(halo[1].astype(F32)) * first

    lane = lax.broadcasted_iota(jnp.int32, (CHUNK, 128), 1)

    @pl.loop(0, rows // CHUNK)
    def _(r):
        base = pl.multiple_of(r * CHUNK, CHUNK)
        span = CHUNK + TAPS_PAD
        window = gated[pl.ds(base, span), :]
        total = jnp.zeros((CHUNK, chans), F32)
        lead = TAPS_PAD - (taps - 1)
        for phase in range(8):
            turned = pltpu.roll(window, span - phase, 0) if phase else window
            for j in range(taps):
                if (lead + j) % 8 == phase:
                    at = lead + j - phase
                    total = total + cw[j : j + 1, :] * turned[at : at + CHUNK]
        conv[pl.ds(base, CHUNK), :] = total
        ssum = jnp.sum(total, axis=1, keepdims=True)
        ssq = jnp.sum(total * total, axis=1, keepdims=True)
        st[pl.ds(base, CHUNK), :] = jnp.where(lane == 0, ssum, jnp.where(lane == 1, ssq, 0.0))

    stats[t] = st[...].T[:8]
    stat_copies = [tp_copy(2, stats.at[t], stats.at[t], d) for d in range(1, T)]
    for copy in stat_copies:
        copy.start()
    direct(0, 1)

    here = pl.ds(pl.multiple_of(t * Q, Q), Q)
    E = S
    expert_iota = lax.broadcasted_iota(jnp.int32, (E, Q), 0)
    id_rows = [ids[k : k + 1, here] for k in range(2)]
    hits = [(expert_iota == id_rows[k]).astype(F32) for k in range(2)]
    upper = (
        lax.broadcasted_iota(jnp.int32, (Q, Q), 0) < lax.broadcasted_iota(jnp.int32, (Q, Q), 1)
    ).astype(BF)
    before = jnp.dot((hits[0] + hits[1]).astype(BF), upper, preferred_element_type=F32)
    slot_rows = [
        id_rows[k].astype(F32) * cap + jnp.sum(before * hits[k], axis=0, keepdims=True)
        for k in range(2)
    ]
    slot_iota = lax.broadcasted_iota(jnp.int32, (slots, Q), 0).astype(F32)
    send_matrix = jnp.where(
        (slot_iota == slot_rows[0]) | (slot_iota == slot_rows[1]), 1.0, 0.0
    ).astype(BF)
    weight = gw[:, here]
    gate_rows = [weight * sigmoid(gap[:, here]), weight * sigmoid(-gap[:, here])]
    table = jnp.concatenate(slot_rows + gate_rows + [jnp.zeros((Q - 4, Q), F32)], axis=0).T
    lane_iota = lax.broadcasted_iota(jnp.int32, (Q, slots), 1).astype(F32)
    for k in range(2):
        place[k] = jnp.where(lane_iota == table[:, k : k + 1], 1.0, 0.0).astype(BF)
    gates = [table[:, 2 + k : 3 + k] for k in range(2)]

    def tp_wait(kind, ref, d):
        remote(ref, ref, tsend.at[kind, d], trecv.at[kind, d], "tp", right).wait_recv()

    for d in range(1, T):
        tp_wait(2, stats.at[lax.rem(t + T - d, T)], d)
    whole = stats[0]
    for b in range(1, T):
        whole = whole + stats[b]
    whole = jnp.concatenate([whole, jnp.zeros((120, rows), F32)], axis=0).T
    mean = whole[:, 0:1] / (chans * T)
    var = whole[:, 1:2] / (chans * T) - mean * mean
    wide = lax.broadcasted_iota(jnp.int32, (rows, 128), 1)
    mv[...] = jnp.where(wide == 0, mean, lax.rsqrt(var + EPS))

    loads[2].wait()

    def project(q, dst):
        at = pl.ds(pl.multiple_of(q * Q, Q), Q)
        stat = mv[at, :]
        normal = (conv[at, :] - stat[:, 0:1]) * stat[:, 1:2] * gain[...] + shift[...]
        act = (normal * sigmoid(normal)).astype(BF)
        for c in range(T):
            cols = pl.ds(c * feats, feats)
            dst[:, cols] = jnp.dot(act, ow[:, cols], preferred_element_type=F32).astype(BF)

    part_copies = []
    for d in (2, 1, 3):
        peer = lax.rem(t + d, T)
        project(peer, part_s.at[d])
        copy = tp_copy(3, part_s.at[d], part_r.at[t], d)
        copy.start()
        part_copies.append(copy)
    project(t, part_r.at[t])

    relay(0)
    loads[1].wait()
    direct(1, 0)
    direct(1, 1)

    for d in range(1, T):
        b = lax.rem(t + T - d, T)
        tp_wait(0, res_r.at[b], d)
        tp_wait(1, mg_r.at[b], d)
        tp_wait(3, part_r.at[b], d)
    square = jnp.zeros((Q, 1), F32)
    for c in range(T):
        cols = pl.ds(c * feats, feats)
        mixed = part_r[0, :, cols].astype(F32)
        for b in range(1, T):
            mixed = mixed + part_r[b, :, cols].astype(F32)
        middle = (res_r[c].astype(F32) + mixed).astype(BF)
        mid[:, cols] = middle
        middle = middle.astype(F32)
        square = square + jnp.sum(middle * middle, axis=1, keepdims=True)
    scale = lax.rsqrt(square / D + EPS)
    for c in range(T):
        cols = pl.ds(c * feats, feats)
        normed = (mid[:, cols].astype(F32) * scale * mg_r[c]).astype(BF)
        sent = jnp.dot(send_matrix, normed, preferred_element_type=F32)
        og[:, :, cols] = sent.reshape(S, cap, feats).astype(BF)
    rc[s] = og[s]

    def sp_exchange(src, dst, send, recv):
        def one(k):
            peer = lax.rem(s + k, S)
            remote(src.at[peer], dst.at[s], send, recv, "sp", peer).start()

        one(S // 2)

        @pl.loop(1, S // 2)
        def _(i):
            one(S // 2 - i)
            one(S // 2 + i)

    def sp_wait(ref, send, recv):
        many = ref.at[pl.ds(0, S - 1)]
        return remote(many, many, send, recv, "tp", right)

    sp_exchange(og, rc, ssend.at[T], srecv.at[T])

    relay(1)
    for c in range(T):
        loads[3 + c].wait()
        direct(2 + c, 0)
        direct(2 + c, 1)
    near_wait(0)
    far_wait(0)
    near_wait(1)
    sp_wait(rc, ssend.at[T], srecv.at[T]).wait_recv()
    for c in range(T):
        cols = pl.ds(c * feats, feats)
        xb[:, cols] = rc[:, :, cols].astype(F32).reshape(slots, feats).astype(BF)

    def expert(b):
        g = jnp.dot(xb[...], wg[b], preferred_element_type=F32)
        u = jnp.dot(xb[...], wu[b], preferred_element_type=F32)
        hid[b] = (g * sigmoid(g) * u).astype(BF)

    relay(2)

    @pl.loop(0, T - 1)
    def _(i):
        expert(lax.rem(t + T - 1 + i, T))

    far_wait(1)
    for c in range(1, T):
        relay(2 + c)
    expert(far)

    for c in range(T):
        near_wait(2 + c)
        far_wait(2 + c)

        @pl.loop(0, 2)
        def _(r, c=c):
            n = slots // 2
            at = pl.ds(pl.multiple_of(r * n, n), n)
            total = jnp.zeros((n, feats), F32)
            for b in range(T):
                term = jnp.dot(hid[b, at, :], wd[c, b], preferred_element_type=F32)
                total = total + term.astype(BF).astype(F32)
            ys[c, pl.ds(r * (S // 2), S // 2)] = total.reshape(S // 2, cap, feats).astype(BF)

        yr[c, s] = ys[c, s]
        sp_exchange(ys.at[c], yr.at[c], ssend.at[c], srecv.at[c])

    for c in range(T):
        sp_wait(yr.at[c], ssend.at[c], srecv.at[c]).wait_recv()
        back = yr[c].astype(F32).reshape(slots, feats).astype(BF)
        cols = pl.ds(c * feats, feats)
        result = mid[:, cols].astype(F32)
        for k in range(2):
            result = result + gates[k] * jnp.dot(place[k], back, preferred_element_type=F32)
        fin[c] = result.astype(BF)
        mine = pl.ds(pl.multiple_of(t * Q, Q), Q)

        @pl.when(t != c)
        def _(c=c):
            remote(fin.at[c], out.at[mine, :], fsend.at[c], frecv.at[t], "tp", c).start()

        @pl.when(t == c)
        def _(c=c):
            out[mine, :] = fin[c]

    for c in range(T):

        @pl.when(t != c)
        def _(c=c):
            remote(fin.at[c], fin.at[c], fsend.at[c], frecv.at[c], "tp", c).wait_send()
            theirs = out.at[pl.ds(c * Q, Q), :]
            remote(theirs, theirs, fsend.at[c], frecv.at[c], "tp", c).wait_recv()

        sp_wait(ys.at[c], ssend.at[c], srecv.at[c]).wait_send()
    sp_wait(og, ssend.at[T], srecv.at[T]).wait_send()
    for copy in halo_copies + res_copies + gain_copies + stat_copies + part_copies:
        copy.wait_send()
    for unit in range(2 + T):
        for h in range(2):
            for i in range(2):
                ring(unit, t, h, True, 2 * h + i).wait_send()
        ring(unit, left, 0, True, 4).wait_send()
        ring(unit, right, 1, True, 5).wait_send()


def shards(
    conv_value,
    conv_gate,
    conv_weight,
    conv_gain,
    conv_shift,
    out_weight,
    residual,
    mix_gain,
    expert_ids,
    group_weight,
    score_gap,
    w_gate,
    w_up,
    w_down,
):
    S, T = lax.axis_size("sp"), lax.axis_size("tp")
    rows, chans = conv_value.shape
    feats = residual.shape[1]
    D = feats * T
    Q = rows // T
    cap = 4 * Q // S
    slots = S * cap
    hidden = w_gate.shape[2]
    vm = pl.BlockSpec(memory_space=pltpu.VMEM)
    hbm = pl.BlockSpec(memory_space=pl.ANY)
    dma = pltpu.SemaphoreType.DMA
    return pl.pallas_call(
        functools.partial(kernel, S, T),
        name="layer",
        out_shape=jax.ShapeDtypeStruct((rows, feats), BF),
        in_specs=[vm] * 5 + [hbm] + [vm] * 5 + [hbm] * 3,
        out_specs=vm,
        scratch_shapes=[
            pltpu.VMEM(out_weight.shape, BF),
            pltpu.VMEM((T, D, hidden), BF),
            pltpu.VMEM((T, D, hidden), BF),
            pltpu.VMEM((T, T, hidden, feats), BF),
            pltpu.VMEM((2, TAPS_PAD, chans), BF),
            pltpu.VMEM((rows + TAPS_PAD, chans), F32),
            pltpu.VMEM((rows, chans), F32),
            pltpu.VMEM((rows, 128), F32),
            pltpu.VMEM((T, 8, rows), F32),
            pltpu.VMEM((rows, 128), F32),
            pltpu.VMEM((T, Q, D), BF),
            pltpu.VMEM((T, Q, D), BF),
            pltpu.VMEM((T, Q, feats), BF),
            pltpu.VMEM((T, 1, feats), F32),
            pltpu.VMEM((Q, D), BF),
            pltpu.VMEM((2, Q, slots), BF),
            pltpu.VMEM((S, cap, D), BF),
            pltpu.VMEM((S, cap, D), BF),
            pltpu.VMEM((slots, D), BF),
            pltpu.VMEM((T, slots, hidden), BF),
            pltpu.VMEM((T, S, cap, feats), BF),
            pltpu.VMEM((T, S, cap, feats), BF),
            pltpu.VMEM((T, Q, feats), BF),
            dma((3 + T,)),
            dma((2,)),
            dma((2,)),
            dma((4, T)),
            dma((4, T)),
            dma((2 + T, 6)),
            dma((2 + T, 6)),
            dma((T + 1,)),
            dma((T + 1,)),
            dma((T,)),
            dma((T,)),
        ],
        compiler_params=pltpu.CompilerParams(
            collective_id=0, has_side_effects=True, vmem_limit_bytes=60 * 1024 * 1024
        ),
    )(
        conv_value,
        conv_gate,
        conv_weight,
        conv_gain.reshape(1, -1),
        conv_shift.reshape(1, -1),
        out_weight,
        residual,
        mix_gain.reshape(1, -1),
        expert_ids.T,
        group_weight.reshape(1, -1),
        score_gap.reshape(1, -1),
        w_gate,
        w_up,
        w_down,
    )


def solution(mesh):
    return jax.shard_map(
        shards,
        mesh=mesh,
        in_specs=(
            P("sp", "tp"),
            P("sp", "tp"),
            P(None, "tp"),
            P("tp"),
            P("tp"),
            P("tp", None),
            P("sp", "tp"),
            P("tp"),
            P("sp", None),
            P("sp"),
            P("sp"),
            P("sp", None, "tp"),
            P("sp", None, "tp"),
            P("sp", "tp", None),
        ),
        out_specs=P("sp", "tp"),
        check_vma=False,
    )
```

time: 336 us -> 196 us (0.58)
  waiting for transfers between devices: 214 us -> 0 us
  Pallas kernels: 0 us -> 194 us
  starting transfers between devices: 48.1 us -> 0 us
  matrix products: 38.2 us -> 0 us
  between operations: 13.4 us -> 0.01 us
  blocking collectives: 11.3 us -> 0 us
  other arithmetic: 4.51 us -> 0 us
    pallas_call x0 -> x1, Pallas kernels: none -> 194 us  [shards(): pl.pallas_call(functools.partial(kernel, S, T), name='layer', out_shape=j...]
    all_gather x4 -> x0, waiting for transfers between devices: 122 us -> none  [the longest x1 52.8 us: shards(): down_full = lax.all_gather(w_down[0], 'tp', axis=0, tiled=False)]
    all_to_all x6 -> x0, waiting for transfers between devices: 89.4 us -> none  [the longest x1 50.5 us: shards(): lax.all_to_all(total.astype(jnp.bfloat16).reshape(sp, capacity, D), 'sp',...]
    all_to_all x6 -> x0, starting transfers between devices: 42.5 us -> none  [the longest x1 10.9 us: shards(): lax.all_to_all(outgoing.reshape(sp, capacity, D), 'sp', split_axis=0, con...]
    dot_general x16 -> x0, matrix products: 38.2 us -> none  [the longest x4 23.4 us: shards(): term = jnp.dot(hidden, down_full[b], preferred_element_type=jnp.float32)]
    all_to_all x1 -> x0, blocking collectives: 11.3 us -> none  [shards(): return lax.all_to_all(result, 'tp', split_axis=1, concat_axis=0, tiled=True)]
    ppermute x2 -> x0, starting transfers between devices: 5.4 us -> none  [passed_along(): lax.ppermute(value, axis, [(source, source + steps) for source in range(l...]
  transfers between devices with their start and end apart: 12 -> 0, of which waited for: 10 -> 0; matrix products, arithmetic and copies ran while one was open for 6% -> 0% of each run, Pallas kernels for 0% -> 0%
where the time goes in v2:
time: 196 us
  Pallas kernels  194 us (99%)
    pallas_call x1, Pallas kernels, shards(): pl.pallas_call(functools.partial(kernel, S, T), name='layer', out_shape=j...  194 us

profile of v2, /device:TPU:24, one launch (start us, length us, event | category | flops | bytes accessed | tf_op | source)
XLA Modules:
  0.0 195.6 jit_solution(5375740029340289010)
XLA Ops:
  0.0 193.7 %layer.1 = bf16[512,512]{1,0:T(8,128)(2,1)} custom-call(bf16[512,256]{1,0:T(8,128)(2,1)} %cv.1, bf16[512,256]{1,0:T(8,128)(2,1)} %cg.1, f32[31,256]{1,0:T(8,128)} %cw.1, f32[1,256]{1,0:T(1,128)} %bitcast.10, f32[1,256]{1,0:T(1,128)} %bitcast.11, bf16[256,2048]{1,0:T(8,128)(2,1)} %ow_hbm.1, bf16[512,512]{1,0:T(8,128)(2,1)} %res.1, f32[1,512]{1,0:T(1,128)} %bitcast.7, ...), custom_call_target="tpu_custom_call" | custom-call | tf_op jit(solution)/shard_map/layer/pallas_call | solution.py:440
  193.7 1.9 copy.16

commit v3 on v2

--- a/solution.py
+++ b/solution.py
@@ -13,6 +13,8 @@
 EPS = 1e-06
 TAPS_PAD = 32
 CHUNK = 64
+XS = 4
+CORES = 2
 
 
 def sigmoid(v):
@@ -47,8 +49,8 @@
     st,
     stats,
     mv,
-    part_s,
-    part_r,
+    act_s,
+    act_r,
     res_r,
     mg_r,
     mid,
@@ -65,6 +67,8 @@
     hrecv,
     tsend,
     trecv,
+    osend,
+    orecv,
     wsend,
     wrecv,
     ssend,
@@ -82,18 +86,25 @@
     cap = og.shape[1]
     hidden = wg.shape[2]
     slots = S * cap
-
-    loads = [
-        pltpu.make_async_copy(wg_hbm.at[0], wg.at[t], loc.at[0]),
-        pltpu.make_async_copy(wu_hbm.at[0], wu.at[t], loc.at[1]),
-        pltpu.make_async_copy(ow_hbm, ow, loc.at[2]),
-    ]
-    for c in range(T):
-        loads.append(
-            pltpu.make_async_copy(
-                wd_hbm.at[0, :, pl.ds(c * feats, feats)], wd.at[c, t], loc.at[3 + c]
+    strip = feats // T
+    core = lax.rem(s, CORES)
+    x = lax.rem(s // CORES, XS)
+    line = s - core - x * CORES
+    x_right, x_left = lax.rem(x + 1, XS), lax.rem(x + XS - 1, XS)
+    x_far = lax.rem(x + 2, XS)
+
+    loads = [pltpu.make_async_copy(ow_hbm, ow.at[t], loc.at[0])]
+    loads.append(pltpu.make_async_copy(wg_hbm.at[0], wg.at[t], loc.at[1]))
+    loads.append(pltpu.make_async_copy(wu_hbm.at[0], wu.at[t], loc.at[2]))
+    for c in range(T):
+        for j in range(T):
+            loads.append(
+                pltpu.make_async_copy(
+                    wd_hbm.at[0, :, pl.ds(j * feats + c * strip, strip)],
+                    wd.at[c, t, :, pl.ds(j * strip, strip)],
+                    loc.at[3 + c * T + j],
+                )
             )
-        )
     for load in loads:
         load.start()
 
@@ -122,21 +133,22 @@
             device_id_type=MESH,
         )
 
+    right, left = lax.rem(t + 1, T), lax.rem(t + T - 1, T)
+    far = lax.rem(t + 2, T)
+
     def tp_copy(kind, src, dst, d):
         return remote(src, dst, tsend.at[kind, d], trecv.at[kind, d], "tp", lax.rem(t + d, T))
 
+    def tp_wait(kind, ref, d):
+        remote(ref, ref, tsend.at[kind, d], trecv.at[kind, d], "tp", right).wait_recv()
+
     def half(unit, block, h):
-        if unit == 0:
-            n = wg.shape[1] // 2
-            return wg.at[block, pl.ds(h * n, n), :]
-        if unit == 1:
-            n = wu.shape[1] // 2
-            return wu.at[block, pl.ds(h * n, n), :]
+        if unit < 4:
+            ref = wg if unit < 2 else wu
+            n = ref.shape[1] // 4
+            return ref.at[block, pl.ds((unit % 2) * 2 * n + h * n, n), :]
         n = hidden // 2
-        return wd.at[unit - 2, block, pl.ds(h * n, n), :]
-
-    right, left = lax.rem(t + 1, T), lax.rem(t + T - 1, T)
-    far = lax.rem(t + 2, T)
+        return wd.at[unit - 4, block, pl.ds(h * n, n), :]
 
     def ring(unit, block, h, to_right, idx):
         ref = half(unit, block, h)
@@ -144,9 +156,13 @@
             ref, ref, wsend.at[unit, idx], wrecv.at[unit, idx], "tp", right if to_right else left
         )
 
-    def direct(unit, h):
-        for to_right in (True, False):
-            ring(unit, t, h, to_right, 2 * h + (0 if to_right else 1)).start()
+    def direct(unit):
+        if unit >= 4:
+            for j in range(T):
+                loads[3 + (unit - 4) * T + j].wait()
+        for h in range(2):
+            ring(unit, t, h, True, 2 * h).start()
+            ring(unit, t, 1 - h, False, 2 * (1 - h) + 1).start()
 
     def direct_wait(unit, h, from_left):
         ring(unit, left if from_left else right, h, True, 2 * h + (0 if from_left else 1)).wait_recv()
@@ -165,33 +181,52 @@
         ring(unit, far, 0, True, 4).wait_recv()
         ring(unit, far, 1, True, 5).wait_recv()
 
-    halo_copies = [
-        remote(
-            src.at[pl.ds(rows - TAPS_PAD, TAPS_PAD), :],
-            halo.at[i],
-            hsend.at[i],
-            hrecv.at[i],
-            "sp",
-            lax.rem(s + 1, S),
+    per = ow.shape[1] // (XS * CORES)
+
+    def piece(block, at_x, at_core, h=None):
+        base = (at_x * CORES + at_core) * per
+        if h is None:
+            return ow.at[block, pl.ds(base, per), :]
+        return ow.at[block, pl.ds(base + h * (per // 2), per // 2), :]
+
+    def from_block(d):
+        return lax.rem(t + T - d, T)
+
+    def share(kind, d, ref, who):
+        return remote(ref, ref, osend.at[kind, d], orecv.at[kind, d], "sp", who)
+
+    to_x_right = line + x_right * CORES + core
+    to_x_left = line + x_left * CORES + core
+    other = line + x * CORES + 1 - core
+    sends = []
+
+    def go(copy):
+        copy.start()
+        sends.append(copy)
+
+    for i, src in enumerate((cv, cg)):
+        go(
+            remote(
+                src.at[pl.ds(rows - TAPS_PAD, TAPS_PAD), :],
+                halo.at[i],
+                hsend.at[i],
+                hrecv.at[i],
+                "sp",
+                lax.rem(s + 1, S),
+            )
         )
-        for i, src in enumerate((cv, cg))
-    ]
-    for copy in halo_copies:
-        copy.start()
-    res_copies, gain_copies = [], []
-    for d in range(1, T):
-        peer = lax.rem(t + d, T)
-        res_copies.append(tp_copy(0, res.at[pl.ds(peer * Q, Q), :], res_r.at[t], d))
-        gain_copies.append(tp_copy(1, mg, mg_r.at[t], d))
-    for copy in res_copies + gain_copies:
-        copy.start()
     loads[0].wait()
-    direct(0, 0)
+    for d in range(1, T):
+        mine = piece(t, x, core)
+        go(tp_copy(3, mine, mine, d))
+    for d in range(1, T):
+        go(tp_copy(0, res.at[pl.ds(lax.rem(t + d, T) * Q, Q), :], res_r.at[t], d))
+        go(tp_copy(1, mg, mg_r.at[t], d))
     res_r[t] = res[pl.ds(t * Q, Q), :]
     mg_r[t] = mg[...]
 
-    for copy in halo_copies:
-        copy.wait_recv()
+    for i in range(2):
+        remote(halo.at[i], halo.at[i], hsend.at[i], hrecv.at[i], "tp", right).wait_recv()
     first = jnp.where(s == 0, 0.0, 1.0).astype(F32)
     gated[:TAPS_PAD, :] = halo[0].astype(F32) * sigmoid(halo[1].astype(F32)) * first
 
@@ -216,10 +251,17 @@
         st[pl.ds(base, CHUNK), :] = jnp.where(lane == 0, ssum, jnp.where(lane == 1, ssq, 0.0))
 
     stats[t] = st[...].T[:8]
-    stat_copies = [tp_copy(2, stats.at[t], stats.at[t], d) for d in range(1, T)]
-    for copy in stat_copies:
-        copy.start()
-    direct(0, 1)
+    for d in range(1, T):
+        go(tp_copy(2, stats.at[t], stats.at[t], d))
+
+    for d in range(1, T):
+        b = from_block(d)
+        tp_wait(3, piece(b, x, core), d)
+        go(share(0, d, piece(b, x, core), to_x_right))
+        go(share(1, d, piece(b, x, core), to_x_left))
+        go(share(4, d, piece(b, x, core), other))
+    loads[1].wait()
+    direct(0)
 
     here = pl.ds(pl.multiple_of(t * Q, Q), Q)
     E = S
@@ -246,11 +288,8 @@
         place[k] = jnp.where(lane_iota == table[:, k : k + 1], 1.0, 0.0).astype(BF)
     gates = [table[:, 2 + k : 3 + k] for k in range(2)]
 
-    def tp_wait(kind, ref, d):
-        remote(ref, ref, tsend.at[kind, d], trecv.at[kind, d], "tp", right).wait_recv()
-
-    for d in range(1, T):
-        tp_wait(2, stats.at[lax.rem(t + T - d, T)], d)
+    for d in range(1, T):
+        tp_wait(2, stats.at[from_block(d)], d)
     whole = stats[0]
     for b in range(1, T):
         whole = whole + stats[b]
@@ -260,42 +299,52 @@
     wide = lax.broadcasted_iota(jnp.int32, (rows, 128), 1)
     mv[...] = jnp.where(wide == 0, mean, lax.rsqrt(var + EPS))
 
-    loads[2].wait()
-
-    def project(q, dst):
+    def activate(q, dst):
         at = pl.ds(pl.multiple_of(q * Q, Q), Q)
         stat = mv[at, :]
         normal = (conv[at, :] - stat[:, 0:1]) * stat[:, 1:2] * gain[...] + shift[...]
-        act = (normal * sigmoid(normal)).astype(BF)
-        for c in range(T):
-            cols = pl.ds(c * feats, feats)
-            dst[:, cols] = jnp.dot(act, ow[:, cols], preferred_element_type=F32).astype(BF)
-
-    part_copies = []
+        dst[...] = (normal * sigmoid(normal)).astype(BF)
+
     for d in (2, 1, 3):
-        peer = lax.rem(t + d, T)
-        project(peer, part_s.at[d])
-        copy = tp_copy(3, part_s.at[d], part_r.at[t], d)
-        copy.start()
-        part_copies.append(copy)
-    project(t, part_r.at[t])
-
-    relay(0)
-    loads[1].wait()
-    direct(1, 0)
-    direct(1, 1)
-
-    for d in range(1, T):
-        b = lax.rem(t + T - d, T)
+        activate(lax.rem(t + d, T), act_s.at[d])
+        go(tp_copy(4, act_s.at[d], act_r.at[t], d))
+    activate(t, act_r.at[t])
+    direct(1)
+
+    for d in range(1, T):
+        b = from_block(d)
+        near = piece(b, x_left, core)
+        share(0, d, near, other).wait_recv()
+        go(share(2, d, piece(b, x_left, core, 0), to_x_right))
+        go(share(5, d, near, other))
+    for d in range(1, T):
+        b = from_block(d)
+        near = piece(b, x_right, core)
+        share(1, d, near, other).wait_recv()
+        go(share(3, d, piece(b, x_right, core, 1), to_x_left))
+        go(share(6, d, near, other))
+    for d in range(1, T):
+        b = from_block(d)
+        share(2, d, piece(b, x_far, core, 0), other).wait_recv()
+        share(3, d, piece(b, x_far, core, 1), other).wait_recv()
+        go(share(7, d, piece(b, x_far, core), other))
+
+    for d in range(1, T):
+        b = from_block(d)
         tp_wait(0, res_r.at[b], d)
         tp_wait(1, mg_r.at[b], d)
-        tp_wait(3, part_r.at[b], d)
+        tp_wait(4, act_r.at[b], d)
+    for i, at_x in enumerate((x, x_left, x_right, x_far)):
+        for d in range(1, T):
+            share(4 + i, d, piece(from_block(d), at_x, 1 - core), other).wait_recv()
+
     square = jnp.zeros((Q, 1), F32)
     for c in range(T):
         cols = pl.ds(c * feats, feats)
-        mixed = part_r[0, :, cols].astype(F32)
-        for b in range(1, T):
-            mixed = mixed + part_r[b, :, cols].astype(F32)
+        mixed = jnp.zeros((Q, feats), F32)
+        for b in range(T):
+            term = jnp.dot(act_r[b], ow[b, :, cols], preferred_element_type=F32)
+            mixed = mixed + term.astype(BF).astype(F32)
         middle = (res_r[c].astype(F32) + mixed).astype(BF)
         mid[:, cols] = middle
         middle = middle.astype(F32)
@@ -326,14 +375,21 @@
 
     sp_exchange(og, rc, ssend.at[T], srecv.at[T])
 
+    relay(0)
+    loads[2].wait()
+    direct(2)
     relay(1)
-    for c in range(T):
-        loads[3 + c].wait()
-        direct(2 + c, 0)
-        direct(2 + c, 1)
-    near_wait(0)
+    direct(3)
+    relay(2)
+    direct(4)
+    relay(3)
+    relay(4)
+    direct(5)
+    direct(6)
+    for unit in range(4):
+        near_wait(unit)
     far_wait(0)
-    near_wait(1)
+    far_wait(1)
     sp_wait(rc, ssend.at[T], srecv.at[T]).wait_recv()
     for c in range(T):
         cols = pl.ds(c * feats, feats)
@@ -344,20 +400,21 @@
         u = jnp.dot(xb[...], wu[b], preferred_element_type=F32)
         hid[b] = (g * sigmoid(g) * u).astype(BF)
 
-    relay(2)
-
     @pl.loop(0, T - 1)
     def _(i):
         expert(lax.rem(t + T - 1 + i, T))
 
-    far_wait(1)
-    for c in range(1, T):
-        relay(2 + c)
+    far_wait(2)
+    far_wait(3)
     expert(far)
 
     for c in range(T):
-        near_wait(2 + c)
-        far_wait(2 + c)
+        if c + 1 < T:
+            relay(5 + c)
+        if c == 0:
+            direct(7)
+        near_wait(4 + c)
+        far_wait(4 + c)
 
         @pl.loop(0, 2)
         def _(r, c=c):
@@ -372,42 +429,35 @@
         yr[c, s] = ys[c, s]
         sp_exchange(ys.at[c], yr.at[c], ssend.at[c], srecv.at[c])
 
+    my_rows = pl.ds(pl.multiple_of(t * Q, Q), Q)
     for c in range(T):
         sp_wait(yr.at[c], ssend.at[c], srecv.at[c]).wait_recv()
         back = yr[c].astype(F32).reshape(slots, feats).astype(BF)
-        cols = pl.ds(c * feats, feats)
-        result = mid[:, cols].astype(F32)
-        for k in range(2):
-            result = result + gates[k] * jnp.dot(place[k], back, preferred_element_type=F32)
-        fin[c] = result.astype(BF)
-        mine = pl.ds(pl.multiple_of(t * Q, Q), Q)
-
-        @pl.when(t != c)
-        def _(c=c):
-            remote(fin.at[c], out.at[mine, :], fsend.at[c], frecv.at[t], "tp", c).start()
-
-        @pl.when(t == c)
-        def _(c=c):
-            out[mine, :] = fin[c]
-
-    for c in range(T):
-
-        @pl.when(t != c)
-        def _(c=c):
-            remote(fin.at[c], fin.at[c], fsend.at[c], frecv.at[c], "tp", c).wait_send()
-            theirs = out.at[pl.ds(c * Q, Q), :]
-            remote(theirs, theirs, fsend.at[c], frecv.at[c], "tp", c).wait_recv()
-
+        picked = [jnp.dot(place[k], back, preferred_element_type=F32) for k in range(2)]
+        added = gates[0] * picked[0] + gates[1] * picked[1]
+        for j in range(T):
+            middle = mid[:, pl.ds(j * feats + c * strip, strip)].astype(F32)
+            fin[c, j] = (middle + added[:, j * strip : (j + 1) * strip]).astype(BF)
+        cols = pl.ds(c * strip, strip)
+        for d in range(1, T):
+            peer = lax.rem(t + d, T)
+            go(remote(fin.at[c, peer], out.at[my_rows, cols], fsend.at[c, d], frecv.at[c, d], "tp", peer))
+        out[my_rows, cols] = fin[c, t]
+
+    for c in range(T):
         sp_wait(ys.at[c], ssend.at[c], srecv.at[c]).wait_send()
     sp_wait(og, ssend.at[T], srecv.at[T]).wait_send()
-    for copy in halo_copies + res_copies + gain_copies + stat_copies + part_copies:
+    for copy in sends:
         copy.wait_send()
-    for unit in range(2 + T):
-        for h in range(2):
-            for i in range(2):
-                ring(unit, t, h, True, 2 * h + i).wait_send()
+    for unit in range(4 + T):
+        for idx in range(4):
+            ring(unit, t, idx // 2, True, idx).wait_send()
         ring(unit, left, 0, True, 4).wait_send()
         ring(unit, right, 1, True, 5).wait_send()
+    for c in range(T):
+        for d in range(1, T):
+            theirs = out.at[pl.ds(from_block(d) * Q, Q), pl.ds(c * strip, strip)]
+            remote(theirs, theirs, fsend.at[c, d], frecv.at[c, d], "tp", right).wait_recv()
 
 
 def shards(
@@ -444,7 +494,7 @@
         in_specs=[vm] * 5 + [hbm] + [vm] * 5 + [hbm] * 3,
         out_specs=vm,
         scratch_shapes=[
-            pltpu.VMEM(out_weight.shape, BF),
+            pltpu.VMEM((T, chans, D), BF),
             pltpu.VMEM((T, D, hidden), BF),
             pltpu.VMEM((T, D, hidden), BF),
             pltpu.VMEM((T, T, hidden, feats), BF),
@@ -454,8 +504,8 @@
             pltpu.VMEM((rows, 128), F32),
             pltpu.VMEM((T, 8, rows), F32),
             pltpu.VMEM((rows, 128), F32),
-            pltpu.VMEM((T, Q, D), BF),
-            pltpu.VMEM((T, Q, D), BF),
+            pltpu.VMEM((T, Q, chans), BF),
+            pltpu.VMEM((T, Q, chans), BF),
             pltpu.VMEM((T, Q, feats), BF),
             pltpu.VMEM((T, 1, feats), F32),
             pltpu.VMEM((Q, D), BF),
@@ -466,18 +516,20 @@
             pltpu.VMEM((T, slots, hidden), BF),
             pltpu.VMEM((T, S, cap, feats), BF),
             pltpu.VMEM((T, S, cap, feats), BF),
-            pltpu.VMEM((T, Q, feats), BF),
-            dma((3 + T,)),
+            pltpu.VMEM((T, T, Q, feats // T), BF),
+            dma((3 + T * T,)),
             dma((2,)),
             dma((2,)),
-            dma((4, T)),
-            dma((4, T)),
-            dma((2 + T, 6)),
-            dma((2 + T, 6)),
+            dma((5, T)),
+            dma((5, T)),
+            dma((8, T)),
+            dma((8, T)),
+            dma((4 + T, 6)),
+            dma((4 + T, 6)),
             dma((T + 1,)),
             dma((T + 1,)),
-            dma((T,)),
-            dma((T,)),
+            dma((T, T)),
+            dma((T, T)),
         ],
         compiler_params=pltpu.CompilerParams(
             collective_id=0, has_side_effects=True, vmem_limit_bytes=60 * 1024 * 1024

time: 196 us -> 166 us (0.85)
  Pallas kernels: 194 us -> 162 us
    pallas_call x1, Pallas kernels: 194 us -> 162 us  [shards(): pl.pallas_call(functools.partial(kernel, S, T), name='layer', out_shape=j...]
where the time goes in v3:
time: 166 us; the launch traced here: 164 us
  Pallas kernels  162 us (98%)
  local copies, waits for them, and re-layouts  1.87 us (1%)
    pallas_call x1, Pallas kernels, shards(): pl.pallas_call(functools.partial(kernel, S, T), name='layer', out_shape=j...  162 us

profile of v3, /device:TPU:24, one launch (start us, length us, event | category | flops | bytes accessed | tf_op | source)
XLA Modules:
  0.0 164.3 jit_solution(11609376113881157024)
XLA Ops:
  0.0 162.4 %layer.1 = bf16[512,512]{1,0:T(8,128)(2,1)} custom-call(bf16[512,256]{1,0:T(8,128)(2,1)} %cv.1, bf16[512,256]{1,0:T(8,128)(2,1)} %cg.1, f32[31,256]{1,0:T(8,128)} %cw.1, f32[1,256]{1,0:T(1,128)} %bitcast.10, f32[1,256]{1,0:T(1,128)} %bitcast.11, bf16[256,2048]{1,0:T(8,128)(2,1)} %ow_hbm.1, bf16[512,512]{1,0:T(8,128)(2,1)} %res.1, f32[1,512]{1,0:T(1,128)} %bitcast.7, ...), custom_call_target="tpu_custom_call" | custom-call | tf_op jit(solution)/shard_map/layer/pallas_call | solution.py:490
  162.4 1.9 %copy.16 = bf16[512,512]{1,0:T(8,128)(2,1)} copy(bf16[512,512]{1,0:T(8,128)(2,1)} %layer.1) | data formatting | bytes 1048576

commit v4 on v3

v4 whole, which is shorter than its diff:
```python
import functools

import jax
import jax.numpy as jnp
from jax import lax
from jax.experimental import pallas as pl
from jax.experimental.pallas import tpu as pltpu
from jax.sharding import PartitionSpec as P

MESH = pl.DeviceIdType.MESH
BF = jnp.bfloat16
F32 = jnp.float32
EPS = 1e-06
TAPS_PAD = 32
CHUNK = 64
CHUNKS = 8
XS = 4
CORES = 2


def sigmoid(v):
    return jax.nn.sigmoid(v)


def kernel(
    S,
    T,
    cv,
    cg,
    cw,
    gain,
    shift,
    ow_hbm,
    res,
    mg,
    ids,
    gw,
    gap,
    wg_hbm,
    wu_hbm,
    wd_hbm,
    out,
    ow,
    wg,
    wu,
    wd,
    halo,
    gated,
    conv,
    st,
    stats,
    mv,
    act_s,
    act_r,
    res_r,
    mg_r,
    mid,
    place,
    og,
    rc,
    xb,
    hid,
    ys,
    yr,
    fin,
    loc,
    hsend,
    hrecv,
    tsend,
    trecv,
    osend,
    orecv,
    wsend,
    wrecv,
    ssend,
    srecv,
    fsend,
    frecv,
):
    t = lax.axis_index("tp")
    s = lax.axis_index("sp")
    rows, chans = cv.shape
    taps = cw.shape[0]
    Q = rows // T
    feats = res.shape[1]
    D = feats * T
    cap = og.shape[1]
    hidden = wg.shape[2]
    chunks = ys.shape[0]
    width = D // chunks
    per_chunk = width // 128
    blocks_by = T // per_chunk
    slots = S * cap
    strip = 128
    core = lax.rem(s, CORES)
    x = lax.rem(s // CORES, XS)
    base = s - core - x * CORES
    depth = S // (XS * CORES)
    z = base // (XS * CORES)
    xp, zp = lax.rem(x, 2), lax.rem(z, 2)
    x_right = base + lax.rem(x + 1, XS) * CORES + core
    x_left = base + lax.rem(x + XS - 1, XS) * CORES + core
    z_right = lax.rem(z + 1, depth) * (XS * CORES) + x * CORES + core
    z_left = lax.rem(z + depth - 1, depth) * (XS * CORES) + x * CORES + core
    other = s + 1 - 2 * core

    loads = [pltpu.make_async_copy(ow_hbm, ow.at[t], loc.at[0])]
    loads.append(pltpu.make_async_copy(wg_hbm.at[0], wg.at[t], loc.at[1]))
    loads.append(pltpu.make_async_copy(wu_hbm.at[0], wu.at[t], loc.at[2]))

    def columns(c, i):
        block = (c % blocks_by) * per_chunk + i
        return block, block * feats + (c // blocks_by) * strip

    for c in range(chunks):
        for i in range(per_chunk):
            loads.append(
                pltpu.make_async_copy(
                    wd_hbm.at[0, :, pl.ds(columns(c, i)[1], strip)],
                    wd.at[c, t, :, pl.ds(i * strip, strip)],
                    loc.at[3 + c * per_chunk + i],
                )
            )
    for load in loads:
        load.start()

    barrier = pltpu.get_barrier_semaphore()

    @pl.loop(1, S)
    def _(k):
        pl.semaphore_signal(
            barrier, inc=1, device_id={"sp": lax.rem(s + k, S)}, device_id_type=MESH
        )

    for d in range(1, T):
        pl.semaphore_signal(
            barrier, inc=1, device_id={"tp": lax.rem(t + d, T)}, device_id_type=MESH
        )
    gated[TAPS_PAD:, :] = cv[...].astype(F32) * sigmoid(cg[...].astype(F32))
    lane = lax.broadcasted_iota(jnp.int32, (CHUNK, 128), 1)

    def conv_rows(r):
        base = r * CHUNK if isinstance(r, int) else pl.multiple_of(r * CHUNK, CHUNK)
        span = CHUNK + TAPS_PAD
        window = gated[pl.ds(base, span), :]
        total = jnp.zeros((CHUNK, chans), F32)
        lead = TAPS_PAD - (taps - 1)
        for phase in range(8):
            turned = pltpu.roll(window, span - phase, 0) if phase else window
            for j in range(taps):
                if (lead + j) % 8 == phase:
                    at = lead + j - phase
                    total = total + cw[j : j + 1, :] * turned[at : at + CHUNK]
        conv[pl.ds(base, CHUNK), :] = total
        ssum = jnp.sum(total, axis=1, keepdims=True)
        ssq = jnp.sum(total * total, axis=1, keepdims=True)
        st[pl.ds(base, CHUNK), :] = jnp.where(lane == 0, ssum, jnp.where(lane == 1, ssq, 0.0))

    @pl.loop(1, rows // CHUNK)
    def _(r):
        conv_rows(r)

    here = pl.ds(pl.multiple_of(t * Q, Q), Q)
    E = S
    expert_iota = lax.broadcasted_iota(jnp.int32, (E, Q), 0)
    id_rows = [ids[k : k + 1, here] for k in range(2)]
    hits = [(expert_iota == id_rows[k]).astype(F32) for k in range(2)]
    upper = (
        lax.broadcasted_iota(jnp.int32, (Q, Q), 0) < lax.broadcasted_iota(jnp.int32, (Q, Q), 1)
    ).astype(BF)
    before = jnp.dot((hits[0] + hits[1]).astype(BF), upper, preferred_element_type=F32)
    slot_rows = [
        id_rows[k].astype(F32) * cap + jnp.sum(before * hits[k], axis=0, keepdims=True)
        for k in range(2)
    ]
    slot_iota = lax.broadcasted_iota(jnp.int32, (slots, Q), 0).astype(F32)
    send_matrix = jnp.where(
        (slot_iota == slot_rows[0]) | (slot_iota == slot_rows[1]), 1.0, 0.0
    ).astype(BF)
    weight = gw[:, here]
    gate_rows = [weight * sigmoid(gap[:, here]), weight * sigmoid(-gap[:, here])]
    table = jnp.concatenate(slot_rows + gate_rows + [jnp.zeros((Q - 4, Q), F32)], axis=0).T
    lane_iota = lax.broadcasted_iota(jnp.int32, (Q, slots), 1).astype(F32)
    for k in range(2):
        place[k] = jnp.where(lane_iota == table[:, k : k + 1], 1.0, 0.0).astype(BF)
    gates = [table[:, 2 + k : 3 + k] for k in range(2)]

    pl.semaphore_wait(barrier, S - 1 + T - 1)

    def remote(src, dst, send, recv, axis, who):
        return pltpu.make_async_remote_copy(
            src_ref=src,
            dst_ref=dst,
            send_sem=send,
            recv_sem=recv,
            device_id={axis: who},
            device_id_type=MESH,
        )

    right, left = lax.rem(t + 1, T), lax.rem(t + T - 1, T)
    far = lax.rem(t + 2, T)

    def tp_copy(kind, src, dst, d):
        return remote(src, dst, tsend.at[kind, d], trecv.at[kind, d], "tp", lax.rem(t + d, T))

    def tp_wait(kind, ref, d):
        remote(ref, ref, tsend.at[kind, d], trecv.at[kind, d], "tp", right).wait_recv()

    def half(unit, block, h):
        if unit < 4:
            ref = wg if unit < 2 else wu
            n = ref.shape[1] // 4
            return ref.at[block, pl.ds((unit % 2) * 2 * n + h * n, n), :]
        n = hidden // 2
        return wd.at[unit - 4, block, pl.ds(h * n, n), :]

    def ring(unit, block, h, to_right, idx):
        ref = half(unit, block, h)
        return remote(
            ref, ref, wsend.at[unit, idx], wrecv.at[unit, idx], "tp", right if to_right else left
        )

    def direct_half(unit, h):
        ring(unit, t, h, True, 2 * h).start()
        ring(unit, t, 1 - h, False, 2 * (1 - h) + 1).start()

    def direct(unit):
        if unit >= 4:
            for i in range(per_chunk):
                loads[3 + (unit - 4) * per_chunk + i].wait()
        direct_half(unit, 0)
        direct_half(unit, 1)

    def direct_wait(unit, h, from_left):
        ring(unit, left if from_left else right, h, True, 2 * h + (0 if from_left else 1)).wait_recv()

    def relay(unit):
        direct_wait(unit, 0, True)
        ring(unit, left, 0, True, 4).start()
        direct_wait(unit, 1, False)
        ring(unit, right, 1, False, 5).start()

    def near_wait(unit):
        direct_wait(unit, 1, True)
        direct_wait(unit, 0, False)

    def far_wait(unit):
        ring(unit, far, 0, True, 4).wait_recv()
        ring(unit, far, 1, True, 5).wait_recv()

    per = ow.shape[1] // 8

    def piece(block, at_x, at_z, at_core, h=None, side=None):
        first = (at_x * 4 + at_z * 2 + at_core) * per
        if h is None:
            return ow.at[block, pl.ds(first, per), :]
        n = per // 2
        if side is None:
            return ow.at[block, pl.ds(first + h * n, n), :]
        return ow.at[block, pl.ds(first + h * n, n), pl.ds(side * (D // 2), D // 2)]

    def from_block(d):
        return lax.rem(t + T - d, T)

    def share(kind, d, ref, who):
        return remote(ref, ref, osend.at[kind, d], orecv.at[kind, d], "sp", who)

    sends = []

    def go(copy):
        copy.start()
        sends.append(copy)

    for i, src in enumerate((cv, cg)):
        go(
            remote(
                src.at[pl.ds(rows - TAPS_PAD, TAPS_PAD), :],
                halo.at[i],
                hsend.at[i],
                hrecv.at[i],
                "sp",
                lax.rem(s + 1, S),
            )
        )
    loads[0].wait()
    for d in range(1, T):
        mine = piece(t, xp, zp, core)
        go(tp_copy(3, mine, mine, d))
    for d in range(1, T):
        go(tp_copy(0, res.at[pl.ds(lax.rem(t + d, T) * Q, Q), :], res_r.at[t], d))
        go(tp_copy(1, mg, mg_r.at[t], d))
    res_r[t] = res[pl.ds(t * Q, Q), :]
    mg_r[t] = mg[...]

    for i in range(2):
        remote(halo.at[i], halo.at[i], hsend.at[i], hrecv.at[i], "tp", right).wait_recv()
    first = jnp.where(s == 0, 0.0, 1.0).astype(F32)
    gated[:TAPS_PAD, :] = halo[0].astype(F32) * sigmoid(halo[1].astype(F32)) * first

    conv_rows(0)
    stats[t] = st[...].T[:8]
    for d in range(1, T):
        go(tp_copy(2, stats.at[t], stats.at[t], d))

    loads[1].wait()
    direct_half(0, 0)

    for d in range(1, T):
        tp_wait(2, stats.at[from_block(d)], d)
    whole = stats[0]
    for b in range(1, T):
        whole = whole + stats[b]
    whole = jnp.concatenate([whole, jnp.zeros((120, rows), F32)], axis=0).T
    mean = whole[:, 0:1] / (chans * T)
    var = whole[:, 1:2] / (chans * T) - mean * mean
    wide = lax.broadcasted_iota(jnp.int32, (rows, 128), 1)
    mv[...] = jnp.where(wide == 0, mean, lax.rsqrt(var + EPS))

    def activate(q, dst):
        at = pl.ds(pl.multiple_of(q * Q, Q), Q)
        stat = mv[at, :]
        normal = (conv[at, :] - stat[:, 0:1]) * stat[:, 1:2] * gain[...] + shift[...]
        dst[...] = (normal * sigmoid(normal)).astype(BF)

    for d in (2, 1, 3):
        activate(lax.rem(t + d, T), act_s.at[d])
        go(tp_copy(4, act_s.at[d], act_r.at[t], d))
    activate(t, act_r.at[t])

    for d in range(1, T):
        b = from_block(d)
        tp_wait(3, piece(b, xp, zp, core), d)
        go(share(0, d, piece(b, xp, zp, core, 0), x_right))
        go(share(1, d, piece(b, xp, zp, core, 1), x_left))
        go(share(2, d, piece(b, xp, zp, core, 0), z_right))
        go(share(3, d, piece(b, xp, zp, core, 1), z_left))
        go(share(8, d, piece(b, xp, zp, core), other))
    direct_half(0, 1)
    direct(1)
    for d in range(1, T):
        b = from_block(d)
        for h in range(2):
            share(h, d, piece(b, 1 - xp, zp, core, h), other).wait_recv()
            share(2 + h, d, piece(b, xp, 1 - zp, core, h), other).wait_recv()
        go(share(4, d, piece(b, xp, 1 - zp, core, 0, 0), x_right))
        go(share(5, d, piece(b, xp, 1 - zp, core, 0, 1), x_left))
        go(share(6, d, piece(b, 1 - xp, zp, core, 1, 0), z_right))
        go(share(7, d, piece(b, 1 - xp, zp, core, 1, 1), z_left))
        go(share(9, d, piece(b, 1 - xp, zp, core), other))
        go(share(10, d, piece(b, xp, 1 - zp, core), other))
    loads[2].wait()
    direct(2)
    for d in range(1, T):
        b = from_block(d)
        for side in range(2):
            share(4 + side, d, piece(b, 1 - xp, 1 - zp, core, 0, side), other).wait_recv()
            share(6 + side, d, piece(b, 1 - xp, 1 - zp, core, 1, side), other).wait_recv()
        go(share(11, d, piece(b, 1 - xp, 1 - zp, core), other))

    for d in range(1, T):
        b = from_block(d)
        tp_wait(0, res_r.at[b], d)
        tp_wait(1, mg_r.at[b], d)
        tp_wait(4, act_r.at[b], d)
    for d in range(1, T):
        for i in range(4):
            at_x = xp if i % 2 == 0 else 1 - xp
            at_z = zp if i < 2 else 1 - zp
            share(8 + i, d, piece(from_block(d), at_x, at_z, 1 - core), other).wait_recv()

    square = jnp.zeros((Q, 1), F32)
    for c in range(T):
        cols = pl.ds(c * feats, feats)
        mixed = jnp.zeros((Q, feats), F32)
        for b in range(T):
            term = jnp.dot(act_r[b], ow[b, :, cols], preferred_element_type=F32)
            mixed = mixed + term.astype(BF).astype(F32)
        middle = (res_r[c].astype(F32) + mixed).astype(BF)
        mid[:, cols] = middle
        middle = middle.astype(F32)
        square = square + jnp.sum(middle * middle, axis=1, keepdims=True)
    scale = lax.rsqrt(square / D + EPS)
    for c in range(T):
        cols = pl.ds(c * feats, feats)
        normed = (mid[:, cols].astype(F32) * scale * mg_r[c]).astype(BF)
        sent = jnp.dot(send_matrix, normed, preferred_element_type=F32)
        og[:, :, cols] = sent.reshape(S, cap, feats).astype(BF)
    rc[s] = og[s]

    def sp_exchange(src, dst, send, recv):
        def one(k):
            peer = lax.rem(s + k, S)
            remote(src.at[peer], dst.at[s], send, recv, "sp", peer).start()

        one(S // 2)

        @pl.loop(1, S // 2)
        def _(i):
            one(S // 2 - i)
            one(S // 2 + i)

    def sp_wait(ref, send, recv):
        many = ref.at[pl.ds(0, S - 1)]
        return remote(many, many, send, recv, "tp", right)

    sp_exchange(og, rc, ssend.at[chunks], srecv.at[chunks])

    relay(0)
    relay(1)
    direct(3)
    direct(4)
    relay(2)
    relay(4)
    relay(3)
    direct(5)
    direct(6)
    for unit in range(4):
        near_wait(unit)
    far_wait(0)
    far_wait(1)
    sp_wait(rc, ssend.at[chunks], srecv.at[chunks]).wait_recv()
    for c in range(T):
        cols = pl.ds(c * feats, feats)
        xb[:, cols] = rc[:, :, cols].astype(F32).reshape(slots, feats).astype(BF)

    def expert(b):
        g = jnp.dot(xb[...], wg[b], preferred_element_type=F32)
        u = jnp.dot(xb[...], wu[b], preferred_element_type=F32)
        hid[b] = (g * sigmoid(g) * u).astype(BF)

    @pl.loop(0, T - 1)
    def _(i):
        expert(lax.rem(t + T - 1 + i, T))

    far_wait(2)
    far_wait(3)
    expert(far)

    for c in range(chunks):
        near_wait(4 + c)
        far_wait(4 + c)

        @pl.loop(0, 2)
        def _(r, c=c):
            n = slots // 2
            at = pl.ds(pl.multiple_of(r * n, n), n)
            total = jnp.zeros((n, width), F32)
            for b in range(T):
                term = jnp.dot(hid[b, at, :], wd[c, b], preferred_element_type=F32)
                total = total + term.astype(BF).astype(F32)
            ys[c, pl.ds(r * (S // 2), S // 2)] = total.reshape(S // 2, cap, width).astype(BF)

        yr[c, s] = ys[c, s]
        sp_exchange(ys.at[c], yr.at[c], ssend.at[c], srecv.at[c])
        if c + 1 < chunks:
            relay(5 + c)
        if c + 3 < chunks:
            direct(7 + c)

    my_rows = pl.ds(pl.multiple_of(t * Q, Q), Q)
    for c in range(chunks):
        sp_wait(yr.at[c], ssend.at[c], srecv.at[c]).wait_recv()
        back = yr[c].astype(F32).reshape(slots, width).astype(BF)
        picked = [jnp.dot(place[k], back, preferred_element_type=F32) for k in range(2)]
        added = gates[0] * picked[0] + gates[1] * picked[1]
        cols = pl.ds((c // blocks_by) * strip, strip)
        for i in range(per_chunk):
            block, at = columns(c, i)
            middle = mid[:, pl.ds(at, strip)].astype(F32)
            fin[c, i] = (middle + added[:, i * strip : (i + 1) * strip]).astype(BF)

            @pl.when(t != block)
            def _(c=c, i=i, block=block, cols=cols):
                remote(
                    fin.at[c, i], out.at[my_rows, cols], fsend.at[c, i], frecv.at[c, t], "tp", block
                ).start()

            @pl.when(t == block)
            def _(c=c, i=i, cols=cols):
                out[my_rows, cols] = fin[c, i]

    for c in range(chunks):
        sp_wait(ys.at[c], ssend.at[c], srecv.at[c]).wait_send()
    sp_wait(og, ssend.at[chunks], srecv.at[chunks]).wait_send()
    for copy in sends:
        copy.wait_send()
    for unit in range(4 + chunks):
        for idx in range(4):
            ring(unit, t, idx // 2, True, idx).wait_send()
        ring(unit, left, 0, True, 4).wait_send()
        ring(unit, right, 1, True, 5).wait_send()
    for c in range(chunks):
        for i in range(per_chunk):
            block = columns(c, i)[0]

            @pl.when(t != block)
            def _(c=c, i=i, block=block):
                remote(fin.at[c, i], fin.at[c, i], fsend.at[c, i], frecv.at[c, block], "tp", block).wait_send()

        cols = pl.ds((c // blocks_by) * strip, strip)
        mine = t // per_chunk == c % blocks_by

        @pl.when(mine)
        def _(c=c, cols=cols):
            for d in range(1, T):
                src = lax.rem(t + d, T)
                theirs = out.at[pl.ds(src * Q, Q), cols]
                remote(theirs, theirs, fsend.at[c, 0], frecv.at[c, src], "tp", src).wait_recv()


def shards(
    conv_value,
    conv_gate,
    conv_weight,
    conv_gain,
    conv_shift,
    out_weight,
    residual,
    mix_gain,
    expert_ids,
    group_weight,
    score_gap,
    w_gate,
    w_up,
    w_down,
):
    S, T = lax.axis_size("sp"), lax.axis_size("tp")
    rows, chans = conv_value.shape
    feats = residual.shape[1]
    D = feats * T
    Q = rows // T
    cap = 4 * Q // S
    slots = S * cap
    hidden = w_gate.shape[2]
    vm = pl.BlockSpec(memory_space=pltpu.VMEM)
    hbm = pl.BlockSpec(memory_space=pl.ANY)
    dma = pltpu.SemaphoreType.DMA
    return pl.pallas_call(
        functools.partial(kernel, S, T),
        name="layer",
        out_shape=jax.ShapeDtypeStruct((rows, feats), BF),
        in_specs=[vm] * 5 + [hbm] + [vm] * 5 + [hbm] * 3,
        out_specs=vm,
        scratch_shapes=[
            pltpu.VMEM((T, chans, D), BF),
            pltpu.VMEM((T, D, hidden), BF),
            pltpu.VMEM((T, D, hidden), BF),
            pltpu.VMEM((CHUNKS, T, hidden, D // CHUNKS), BF),
            pltpu.VMEM((2, TAPS_PAD, chans), BF),
            pltpu.VMEM((rows + TAPS_PAD, chans), F32),
            pltpu.VMEM((rows, chans), F32),
            pltpu.VMEM((rows, 128), F32),
            pltpu.VMEM((T, 8, rows), F32),
            pltpu.VMEM((rows, 128), F32),
            pltpu.VMEM((T, Q, chans), BF),
            pltpu.VMEM((T, Q, chans), BF),
            pltpu.VMEM((T, Q, feats), BF),
            pltpu.VMEM((T, 1, feats), F32),
            pltpu.VMEM((Q, D), BF),
            pltpu.VMEM((2, Q, slots), BF),
            pltpu.VMEM((S, cap, D), BF),
            pltpu.VMEM((S, cap, D), BF),
            pltpu.VMEM((slots, D), BF),
            pltpu.VMEM((T, slots, hidden), BF),
            pltpu.VMEM((CHUNKS, S, cap, D // CHUNKS), BF),
            pltpu.VMEM((CHUNKS, S, cap, D // CHUNKS), BF),
            pltpu.VMEM((CHUNKS, D // CHUNKS // 128, Q, 128), BF),
            dma((3 + D // 128,)),
            dma((2,)),
            dma((2,)),
            dma((5, T)),
            dma((5, T)),
            dma((12, T)),
            dma((12, T)),
            dma((4 + CHUNKS, 6)),
            dma((4 + CHUNKS, 6)),
            dma((CHUNKS + 1,)),
            dma((CHUNKS + 1,)),
            dma((CHUNKS, 2)),
            dma((CHUNKS, T)),
        ],
        compiler_params=pltpu.CompilerParams(
            collective_id=0, has_side_effects=True, vmem_limit_bytes=60 * 1024 * 1024
        ),
    )(
        conv_value,
        conv_gate,
        conv_weight,
        conv_gain.reshape(1, -1),
        conv_shift.reshape(1, -1),
        out_weight,
        residual,
        mix_gain.reshape(1, -1),
        expert_ids.T,
        group_weight.reshape(1, -1),
        score_gap.reshape(1, -1),
        w_gate,
        w_up,
        w_down,
    )


def solution(mesh):
    return jax.shard_map(
        shards,
        mesh=mesh,
        in_specs=(
            P("sp", "tp"),
            P("sp", "tp"),
            P(None, "tp"),
            P("tp"),
            P("tp"),
            P("tp", None),
            P("sp", "tp"),
            P("tp"),
            P("sp", None),
            P("sp"),
            P("sp"),
            P("sp", None, "tp"),
            P("sp", None, "tp"),
            P("sp", "tp", None),
        ),
        out_specs=P("sp", "tp"),
        check_vma=False,
    )
```

time: 166 us -> 159 us (0.958)
  Pallas kernels: 162 us -> 157 us
    pallas_call x1, Pallas kernels: 162 us -> 157 us  [shards(): pl.pallas_call(functools.partial(kernel, S, T), name='layer', out_shape=j...]
where the time goes in v4:
time: 159 us
  Pallas kernels  157 us (99%)
  local copies, waits for them, and re-layouts  1.87 us (1%)
    pallas_call x1, Pallas kernels, shards(): pl.pallas_call(functools.partial(kernel, S, T), name='layer', out_shape=j...  157 us

profile of v4, /device:TPU:24, one launch (start us, length us, event | category | flops | bytes accessed | tf_op | source)
XLA Modules:
  0.0 158.9 jit_solution(9714601869937059083)
XLA Ops:
  0.0 157.0 %layer.1 = bf16[512,512]{1,0:T(8,128)(2,1)} custom-call(bf16[512,256]{1,0:T(8,128)(2,1)} %cv.1, bf16[512,256]{1,0:T(8,128)(2,1)} %cg.1, f32[31,256]{1,0:T(8,128)} %cw.1, f32[1,256]{1,0:T(1,128)} %bitcast.10, f32[1,256]{1,0:T(1,128)} %bitcast.11, bf16[256,2048]{1,0:T(8,128)(2,1)} %ow_hbm.1, bf16[512,512]{1,0:T(8,128)(2,1)} %res.1, f32[1,512]{1,0:T(1,128)} %bitcast.7, ...), custom_call_target="tpu_custom_call" | custom-call | tf_op jit(solution)/shard_map/layer/pallas_call | solution.py:538
  157.0 1.9 %copy.16 = bf16[512,512]{1,0:T(8,128)(2,1)} copy(bf16[512,512]{1,0:T(8,128)(2,1)} %layer.1) | data formatting | bytes 1048576

commit v5 on v4

--- a/solution.py
+++ b/solution.py
@@ -25,17 +25,17 @@
 def kernel(
     S,
     T,
-    cv,
-    cg,
-    cw,
-    gain,
-    shift,
+    cv_in,
+    cg_in,
+    cw_in,
+    gain_in,
+    shift_in,
     ow_hbm,
-    res,
-    mg,
-    ids,
-    gw,
-    gap,
+    res_in,
+    mg_in,
+    ids_in,
+    gw_in,
+    gap_in,
     wg_hbm,
     wu_hbm,
     wd_hbm,
@@ -76,6 +76,17 @@
     srecv,
     fsend,
     frecv,
+    cv,
+    cg,
+    cw,
+    gain,
+    shift,
+    res,
+    mg,
+    ids,
+    gw,
+    gap,
+    opsem,
 ):
     t = lax.axis_index("tp")
     s = lax.axis_index("sp")
@@ -97,14 +108,44 @@
     base = s - core - x * CORES
     depth = S // (XS * CORES)
     z = base // (XS * CORES)
-    xp, zp = lax.rem(x, 2), lax.rem(z, 2)
-    x_right = base + lax.rem(x + 1, XS) * CORES + core
-    x_left = base + lax.rem(x + XS - 1, XS) * CORES + core
+    zp = lax.rem(z, 2)
     z_right = lax.rem(z + 1, depth) * (XS * CORES) + x * CORES + core
     z_left = lax.rem(z + depth - 1, depth) * (XS * CORES) + x * CORES + core
     other = s + 1 - 2 * core
 
+    barrier = pltpu.get_barrier_semaphore()
+
+    @pl.loop(1, S)
+    def _(k):
+        pl.semaphore_signal(
+            barrier, inc=1, device_id={"sp": lax.rem(s + k, S)}, device_id_type=MESH
+        )
+
+    for d in range(1, T):
+        pl.semaphore_signal(
+            barrier, inc=1, device_id={"tp": lax.rem(t + d, T)}, device_id_type=MESH
+        )
     loads = [pltpu.make_async_copy(ow_hbm, ow.at[t], loc.at[0])]
+    operands = [
+        pltpu.make_async_copy(src, dst, opsem.at[i])
+        for i, (src, dst) in enumerate(
+            (
+                (cv_in, cv),
+                (cg_in, cg),
+                (mg_in, mg),
+                (cw_in, cw),
+                (gain_in, gain),
+                (shift_in, shift),
+                (ids_in, ids),
+                (gw_in, gw),
+                (gap_in, gap),
+                (res_in, res),
+            )
+        )
+    ]
+    loads[0].start()
+    for load in operands:
+        load.start()
     loads.append(pltpu.make_async_copy(wg_hbm.at[0], wg.at[t], loc.at[1]))
     loads.append(pltpu.make_async_copy(wu_hbm.at[0], wu.at[t], loc.at[2]))
 
@@ -121,21 +162,117 @@
                     loc.at[3 + c * per_chunk + i],
                 )
             )
-    for load in loads:
+    for load in loads[1:]:
         load.start()
 
-    barrier = pltpu.get_barrier_semaphore()
-
-    @pl.loop(1, S)
-    def _(k):
-        pl.semaphore_signal(
-            barrier, inc=1, device_id={"sp": lax.rem(s + k, S)}, device_id_type=MESH
+    pl.semaphore_wait(barrier, S - 1 + T - 1)
+    for load in operands:
+        load.wait()
+
+    def remote(src, dst, send, recv, axis, who):
+        return pltpu.make_async_remote_copy(
+            src_ref=src,
+            dst_ref=dst,
+            send_sem=send,
+            recv_sem=recv,
+            device_id={axis: who},
+            device_id_type=MESH,
         )
 
+    right, left = lax.rem(t + 1, T), lax.rem(t + T - 1, T)
+    far = lax.rem(t + 2, T)
+
+    def tp_copy(kind, src, dst, d):
+        return remote(src, dst, tsend.at[kind, d], trecv.at[kind, d], "tp", lax.rem(t + d, T))
+
+    def tp_wait(kind, ref, d):
+        remote(ref, ref, tsend.at[kind, d], trecv.at[kind, d], "tp", right).wait_recv()
+
+    def half(unit, block, h):
+        if unit < 4:
+            ref = wg if unit < 2 else wu
+            n = ref.shape[1] // 4
+            return ref.at[block, pl.ds((unit % 2) * 2 * n + h * n, n), :]
+        n = hidden // 2
+        return wd.at[unit - 4, block, pl.ds(h * n, n), :]
+
+    def ring(unit, block, h, to_right, idx):
+        ref = half(unit, block, h)
+        return remote(
+            ref, ref, wsend.at[unit, idx], wrecv.at[unit, idx], "tp", right if to_right else left
+        )
+
+    def direct_half(unit, h):
+        ring(unit, t, h, True, 2 * h).start()
+        ring(unit, t, 1 - h, False, 2 * (1 - h) + 1).start()
+
+    def direct(unit):
+        if unit >= 4:
+            for i in range(per_chunk):
+                loads[3 + (unit - 4) * per_chunk + i].wait()
+        direct_half(unit, 0)
+        direct_half(unit, 1)
+
+    def direct_wait(unit, h, from_left):
+        ring(unit, left if from_left else right, h, True, 2 * h + (0 if from_left else 1)).wait_recv()
+
+    def relay(unit):
+        direct_wait(unit, 0, True)
+        ring(unit, left, 0, True, 4).start()
+        direct_wait(unit, 1, False)
+        ring(unit, right, 1, False, 5).start()
+
+    def near_wait(unit):
+        direct_wait(unit, 1, True)
+        direct_wait(unit, 0, False)
+
+    def far_wait(unit):
+        ring(unit, far, 0, True, 4).wait_recv()
+        ring(unit, far, 1, True, 5).wait_recv()
+
+    per = ow.shape[1] // (XS * 2 * CORES)
+
+    def piece(block, at_x, at_z, at_core, h=None):
+        rows_at = pl.ds(((at_x * 2 + at_z) * CORES + at_core) * per, per)
+        if h is None:
+            return ow.at[block, rows_at, :]
+        return ow.at[block, rows_at, pl.ds(h * (D // 2), D // 2)]
+
+    def x_back(r):
+        return lax.rem(x + XS - r, XS)
+
+    def from_block(d):
+        return lax.rem(t + T - d, T)
+
+    def share(kind, d, ref, who):
+        return remote(ref, ref, osend.at[kind, d], orecv.at[kind, d], "sp", who)
+
+    sends = []
+
+    def go(copy):
+        copy.start()
+        sends.append(copy)
+
+    for i, src in enumerate((cv, cg)):
+        go(
+            remote(
+                src.at[pl.ds(rows - TAPS_PAD, TAPS_PAD), :],
+                halo.at[i],
+                hsend.at[i],
+                hrecv.at[i],
+                "sp",
+                lax.rem(s + 1, S),
+            )
+        )
+    loads[0].wait()
+    for d in (1, 3, 2):
+        mine = piece(t, x, zp, core)
+        go(tp_copy(3, mine, mine, d))
     for d in range(1, T):
-        pl.semaphore_signal(
-            barrier, inc=1, device_id={"tp": lax.rem(t + d, T)}, device_id_type=MESH
-        )
+        go(tp_copy(1, mg, mg_r.at[t], d))
+    res_r[t] = res[pl.ds(t * Q, Q), :]
+    mg_r[t] = mg[...]
+
     gated[TAPS_PAD:, :] = cv[...].astype(F32) * sigmoid(cg[...].astype(F32))
     lane = lax.broadcasted_iota(jnp.int32, (CHUNK, 128), 1)
 
@@ -185,113 +322,6 @@
         place[k] = jnp.where(lane_iota == table[:, k : k + 1], 1.0, 0.0).astype(BF)
     gates = [table[:, 2 + k : 3 + k] for k in range(2)]
 
-    pl.semaphore_wait(barrier, S - 1 + T - 1)
-
-    def remote(src, dst, send, recv, axis, who):
-        return pltpu.make_async_remote_copy(
-            src_ref=src,
-            dst_ref=dst,
-            send_sem=send,
-            recv_sem=recv,
-            device_id={axis: who},
-            device_id_type=MESH,
-        )
-
-    right, left = lax.rem(t + 1, T), lax.rem(t + T - 1, T)
-    far = lax.rem(t + 2, T)
-
-    def tp_copy(kind, src, dst, d):
-        return remote(src, dst, tsend.at[kind, d], trecv.at[kind, d], "tp", lax.rem(t + d, T))
-
-    def tp_wait(kind, ref, d):
-        remote(ref, ref, tsend.at[kind, d], trecv.at[kind, d], "tp", right).wait_recv()
-
-    def half(unit, block, h):
-        if unit < 4:
-            ref = wg if unit < 2 else wu
-            n = ref.shape[1] // 4
-            return ref.at[block, pl.ds((unit % 2) * 2 * n + h * n, n), :]
-        n = hidden // 2
-        return wd.at[unit - 4, block, pl.ds(h * n, n), :]
-
-    def ring(unit, block, h, to_right, idx):
-        ref = half(unit, block, h)
-        return remote(
-            ref, ref, wsend.at[unit, idx], wrecv.at[unit, idx], "tp", right if to_right else left
-        )
-
-    def direct_half(unit, h):
-        ring(unit, t, h, True, 2 * h).start()
-        ring(unit, t, 1 - h, False, 2 * (1 - h) + 1).start()
-
-    def direct(unit):
-        if unit >= 4:
-            for i in range(per_chunk):
-                loads[3 + (unit - 4) * per_chunk + i].wait()
-        direct_half(unit, 0)
-        direct_half(unit, 1)
-
-    def direct_wait(unit, h, from_left):
-        ring(unit, left if from_left else right, h, True, 2 * h + (0 if from_left else 1)).wait_recv()
-
-    def relay(unit):
-        direct_wait(unit, 0, True)
-        ring(unit, left, 0, True, 4).start()
-        direct_wait(unit, 1, False)
-        ring(unit, right, 1, False, 5).start()
-
-    def near_wait(unit):
-        direct_wait(unit, 1, True)
-        direct_wait(unit, 0, False)
-
-    def far_wait(unit):
-        ring(unit, far, 0, True, 4).wait_recv()
-        ring(unit, far, 1, True, 5).wait_recv()
-
-    per = ow.shape[1] // 8
-
-    def piece(block, at_x, at_z, at_core, h=None, side=None):
-        first = (at_x * 4 + at_z * 2 + at_core) * per
-        if h is None:
-            return ow.at[block, pl.ds(first, per), :]
-        n = per // 2
-        if side is None:
-            return ow.at[block, pl.ds(first + h * n, n), :]
-        return ow.at[block, pl.ds(first + h * n, n), pl.ds(side * (D // 2), D // 2)]
-
-    def from_block(d):
-        return lax.rem(t + T - d, T)
-
-    def share(kind, d, ref, who):
-        return remote(ref, ref, osend.at[kind, d], orecv.at[kind, d], "sp", who)
-
-    sends = []
-
-    def go(copy):
-        copy.start()
-        sends.append(copy)
-
-    for i, src in enumerate((cv, cg)):
-        go(
-            remote(
-                src.at[pl.ds(rows - TAPS_PAD, TAPS_PAD), :],
-                halo.at[i],
-                hsend.at[i],
-                hrecv.at[i],
-                "sp",
-                lax.rem(s + 1, S),
-            )
-        )
-    loads[0].wait()
-    for d in range(1, T):
-        mine = piece(t, xp, zp, core)
-        go(tp_copy(3, mine, mine, d))
-    for d in range(1, T):
-        go(tp_copy(0, res.at[pl.ds(lax.rem(t + d, T) * Q, Q), :], res_r.at[t], d))
-        go(tp_copy(1, mg, mg_r.at[t], d))
-    res_r[t] = res[pl.ds(t * Q, Q), :]
-    mg_r[t] = mg[...]
-
     for i in range(2):
         remote(halo.at[i], halo.at[i], hsend.at[i], hrecv.at[i], "tp", right).wait_recv()
     first = jnp.where(s == 0, 0.0, 1.0).astype(F32)
@@ -304,6 +334,22 @@
 
     loads[1].wait()
     direct_half(0, 0)
+
+    def to_z(d, r):
+        block, at_x = from_block(d), x_back(r)
+        go(share(3 + 2 * r, d, piece(block, at_x, zp, core, 0), z_right))
+        go(share(4 + 2 * r, d, piece(block, at_x, zp, core, 1), z_left))
+        go(share(11 + 2 * r, d, piece(block, at_x, zp, core), other))
+
+    def pass_on(d):
+        mine = piece(from_block(d), x, zp, core)
+        tp_wait(3, mine, d)
+        for r in range(1, XS):
+            go(share(r - 1, d, mine, base + lax.rem(x + r, XS) * CORES + core))
+        to_z(d, 0)
+
+    pass_on(1)
+    pass_on(3)
 
     for d in range(1, T):
         tp_wait(2, stats.at[from_block(d)], d)
@@ -326,36 +372,24 @@
         activate(lax.rem(t + d, T), act_s.at[d])
         go(tp_copy(4, act_s.at[d], act_r.at[t], d))
     activate(t, act_r.at[t])
-
     for d in range(1, T):
-        b = from_block(d)
-        tp_wait(3, piece(b, xp, zp, core), d)
-        go(share(0, d, piece(b, xp, zp, core, 0), x_right))
-        go(share(1, d, piece(b, xp, zp, core, 1), x_left))
-        go(share(2, d, piece(b, xp, zp, core, 0), z_right))
-        go(share(3, d, piece(b, xp, zp, core, 1), z_left))
-        go(share(8, d, piece(b, xp, zp, core), other))
+        go(tp_copy(0, res.at[pl.ds(lax.rem(t + d, T) * Q, Q), :], res_r.at[t], d))
+
+    pass_on(2)
     direct_half(0, 1)
     direct(1)
-    for d in range(1, T):
-        b = from_block(d)
-        for h in range(2):
-            share(h, d, piece(b, 1 - xp, zp, core, h), other).wait_recv()
-            share(2 + h, d, piece(b, xp, 1 - zp, core, h), other).wait_recv()
-        go(share(4, d, piece(b, xp, 1 - zp, core, 0, 0), x_right))
-        go(share(5, d, piece(b, xp, 1 - zp, core, 0, 1), x_left))
-        go(share(6, d, piece(b, 1 - xp, zp, core, 1, 0), z_right))
-        go(share(7, d, piece(b, 1 - xp, zp, core, 1, 1), z_left))
-        go(share(9, d, piece(b, 1 - xp, zp, core), other))
-        go(share(10, d, piece(b, xp, 1 - zp, core), other))
+    for r in (1, 3, 2):
+        for d in (1, 3, 2):
+            share(r - 1, d, piece(from_block(d), x_back(r), zp, core), other).wait_recv()
+            to_z(d, r)
     loads[2].wait()
     direct(2)
-    for d in range(1, T):
-        b = from_block(d)
-        for side in range(2):
-            share(4 + side, d, piece(b, 1 - xp, 1 - zp, core, 0, side), other).wait_recv()
-            share(6 + side, d, piece(b, 1 - xp, 1 - zp, core, 1, side), other).wait_recv()
-        go(share(11, d, piece(b, 1 - xp, 1 - zp, core), other))
+    for r in (0, 1, 3, 2):
+        for d in (1, 3, 2):
+            block, at_x = from_block(d), x_back(r)
+            for h in range(2):
+                share(3 + 2 * r + h, d, piece(block, at_x, 1 - zp, core, h), other).wait_recv()
+            go(share(12 + 2 * r, d, piece(block, at_x, 1 - zp, core), other))
 
     for d in range(1, T):
         b = from_block(d)
@@ -363,10 +397,12 @@
         tp_wait(1, mg_r.at[b], d)
         tp_wait(4, act_r.at[b], d)
     for d in range(1, T):
-        for i in range(4):
-            at_x = xp if i % 2 == 0 else 1 - xp
-            at_z = zp if i < 2 else 1 - zp
-            share(8 + i, d, piece(from_block(d), at_x, at_z, 1 - core), other).wait_recv()
+        for r in range(XS):
+            for far_z in range(2):
+                at_z = 1 - zp if far_z else zp
+                share(
+                    11 + 2 * r + far_z, d, piece(from_block(d), x_back(r), at_z, 1 - core), other
+                ).wait_recv()
 
     square = jnp.zeros((Q, 1), F32)
     for c in range(T):
@@ -539,7 +575,7 @@
         functools.partial(kernel, S, T),
         name="layer",
         out_shape=jax.ShapeDtypeStruct((rows, feats), BF),
-        in_specs=[vm] * 5 + [hbm] + [vm] * 5 + [hbm] * 3,
+        in_specs=[hbm] * 14,
         out_specs=vm,
         scratch_shapes=[
             pltpu.VMEM((T, chans, D), BF),
@@ -570,14 +606,25 @@
             dma((2,)),
             dma((5, T)),
             dma((5, T)),
-            dma((12, T)),
-            dma((12, T)),
+            dma((19, T)),
+            dma((19, T)),
             dma((4 + CHUNKS, 6)),
             dma((4 + CHUNKS, 6)),
             dma((CHUNKS + 1,)),
             dma((CHUNKS + 1,)),
             dma((CHUNKS, 2)),
             dma((CHUNKS, T)),
+            pltpu.VMEM((rows, chans), BF),
+            pltpu.VMEM((rows, chans), BF),
+            pltpu.VMEM(conv_weight.shape, F32),
+            pltpu.VMEM((1, chans), F32),
+            pltpu.VMEM((1, chans), F32),
+            pltpu.VMEM((rows, feats), BF),
+            pltpu.VMEM((1, feats), F32),
+            pltpu.VMEM((2, rows), jnp.int32),
+            pltpu.VMEM((1, rows), F32),
+            pltpu.VMEM((1, rows), F32),
+            dma((10,)),
         ],
         compiler_params=pltpu.CompilerParams(
             collective_id=0, has_side_effects=True, vmem_limit_bytes=60 * 1024 * 1024

time: 159 us -> 157 us (0.987)
  Pallas kernels: 157 us -> 155 us
    pallas_call x1, Pallas kernels: 157 us -> 155 us  [shards(): pl.pallas_call(functools.partial(kernel, S, T), name='layer', out_shape=j...]
where the time goes in v5:
time: 157 us; the launch traced here: 156 us
  Pallas kernels  155 us (99%)
  local copies, waits for them, and re-layouts  1.87 us (1%)
    pallas_call x1, Pallas kernels, shards(): pl.pallas_call(functools.partial(kernel, S, T), name='layer', out_shape=j...  155 us

profile of v5, /device:TPU:24, one launch (start us, length us, event | category | flops | bytes accessed | tf_op | source)
XLA Modules:
  0.0 156.4 jit_solution(2244686295822013308)
XLA Ops:
  0.0 154.5 %layer.1 = bf16[512,512]{1,0:T(8,128)(2,1)} custom-call(bf16[512,256]{1,0:T(8,128)(2,1)} %cv_in.1, bf16[512,256]{1,0:T(8,128)(2,1)} %cg_in.1, f32[31,256]{1,0:T(8,128)} %cw_in.1, f32[1,256]{1,0:T(1,128)} %bitcast.10, f32[1,256]{1,0:T(1,128)} %bitcast.11, bf16[256,2048]{1,0:T(8,128)(2,1)} %ow_hbm.1, bf16[512,512]{1,0:T(8,128)(2,1)} %res_in.1, ...), custom_call_target="tpu_custom_call" | custom-call | tf_op jit(solution)/shard_map/layer/pallas_call | solution.py:574
  154.5 1.9 %copy.16 = bf16[512,512]{1,0:T(8,128)(2,1)} copy(bf16[512,512]{1,0:T(8,128)(2,1)} %layer.1) | data formatting | bytes 1048576
